TPU v7x, 512 devices: a whole 4x8x8 slice. The times are simulated.
512 devices in a mesh: sp: 128 (over z, y, core), tp: 4 (over x).
Axes of the slice: x: 4, y: 8, z: 8, core: 2. Of those that a mesh axis runs over, the one named last changes fastest.
Arguments:
- tokens: bfloat16 [24576, 2048], P('sp', 'tp'), may hold values from -6 to 6
- norm_gain: float32 [2048], replicated, may hold values from 0.1 to 1.9
- query_weight: bfloat16 [2048, 512], P('sp', 'tp'), may hold values from -0.125 to 0.125
- key_weight: bfloat16 [2048, 512], P('sp', 'tp'), may hold values from -0.125 to 0.125
- value_weight: bfloat16 [2048, 512], P('sp', 'tp'), may hold values from -0.125 to 0.125
- decay_weight: bfloat16 [2048, 512], P('sp', 'tp'), may hold values from -0.09375 to 0.09375
- removal_weight: bfloat16 [2048, 512], P('sp', 'tp'), may hold values from -0.125 to 0.125
- gate_weight: bfloat16 [2048, 512], P('sp', 'tp'), may hold values from -0.125 to 0.125
- key_gain: float32 [512], P('tp'), may hold values from 0.1 to 1.9
- removal_gain: float32 [512], P('tp'), may hold values from 0.1 to 1.9
- removal_bias: float32 [512], P('tp'), may hold values from -9 to 1
- decay_bias: float32 [512], P('tp'), may hold values from -12.7 to -1.8
- decay_extra: float32 [24576, 512], P('sp', 'tp'), may hold values from 0 to 0.7
- scan_norm_gain: float32 [512], P('tp'), may hold values from 0.1 to 1.9
- conv_value_weight: bfloat16 [2048, 512], P('sp', 'tp'), may hold values from -0.125 to 0.125
- conv_gate_weight: bfloat16 [2048, 512], P('sp', 'tp'), may hold values from -0.125 to 0.125
- conv_kernel: float32 [31, 512], P(None, 'tp'), may hold values from -2 to 2
- conv_bias: float32 [512], P('tp'), may hold values from -2 to 3
- conv_norm_gain: float32 [512], P('tp'), may hold values from 0.1 to 1.9
- out_scan_weight: bfloat16 [512, 2048], P('tp', 'sp'), may hold values from -0.1875 to 0.1875
- out_conv_weight: bfloat16 [512, 2048], P('tp', 'sp'), may hold values from -0.1875 to 0.1875
Outputs:
- mixed: bfloat16 [24576, 2048], P('sp', 'tp')
All inputs are finite; a program needn't handle non-finite values.
Results may differ from a plain program's by a relative error of at most 0.0073.
Values may be sent and summed in bfloat16 or wider, within the bound.
A program may use at most 64 MiB of HBM per device.

v0:
```python
import jax
import jax.numpy as jnp
from jax import lax
from jax.sharding import Mesh
from jax.sharding import PartitionSpec as P

HEAD_SIZE = 64
CONV_K = 31
BLOCK = 32
SP = ("sp_0", "sp_1", "sp_2")


exact_setting = lax.Precision.HIGHEST


def neutral_like(x, identity):
    return jax.tree.map(
        lambda part, zero: jnp.zeros_like(part) + jnp.asarray(zero, part.dtype), x, identity
    )


def collected_together(x, axis):
    leaves = jax.tree.leaves(x)
    sequence = sorted(range(len(leaves)), key=lambda k: -leaves[k].size)
    width = (1, *leaves[sequence[0]].shape)[-1]
    lines = [
        jnp.pad(leaves[k].reshape(-1), (0, -leaves[k].size % width)).reshape(-1, width)
        for k in sequence
    ]
    both, at, found = (lax.all_gather(jnp.concatenate(lines), axis), 0, {})
    for k, line in zip(sequence, lines):
        slab = both[:, at : at + len(line)].reshape(len(both), -1)
        found[k] = slab[:, : leaves[k].size].reshape(-1, *leaves[k].shape)
        at += len(line)
    numbers = iter(range(len(leaves)))
    return jax.tree.map(lambda _: found[next(numbers)], x)


def carried_in(x, axes, combine, identity):
    before = start = neutral_like(x, identity)
    total = x
    for axis in reversed(axes):
        size, here = (lax.axis_size(axis), lax.axis_index(axis))
        pieces = collected_together(total, axis)
        inside, total = (start, start)
        for k in range(size):
            passed = k < here
            total = combine(total, jax.tree.map(lambda part: part[k], pieces))
            inside = jax.tree.map(lambda new, old: jnp.where(passed, new, old), total, inside)
        before = combine(inside, before)
    return before


def shifted(value, axis, steps):
    count = lax.axis_size(axis)
    leading, last = (max(0, -steps), min(count, count - steps))
    return lax.ppermute(value, axis, [(source, source + steps) for source in range(leading, last)])


def copy_for_each(x, axis):
    size = lax.axis_size(axis)
    return lax.all_to_all(jnp.broadcast_to(x[None], (size, *x.shape)), axis, 0, 0, tiled=True)


def taken_together(x, axis):
    everything = copy_for_each(x, axis)
    return jnp.sum(everything, axis=0)


def in_one(arrays, axis):
    vector, at, finished = (jnp.concatenate([a.reshape(-1) for a in arrays]), 0, [])
    total = taken_together(vector, axis)
    for a in arrays:
        finished.append(total[at : at + a.size].reshape(a.shape))
        at += a.size
    return tuple(finished)


def laid_out(pieces, dim):
    pieces = jnp.moveaxis(pieces, 0, dim)
    shape = pieces.shape
    return pieces.reshape(*shape[:dim], shape[dim] * shape[dim + 1], *shape[dim + 2 :])


def gather_directly(x, axis, dim):
    pieces = copy_for_each(x, axis)
    return laid_out(pieces, dim)


def side_by_side(arrays, axis, dim, along):
    both = jnp.concatenate(arrays, axis=along)
    filled, at, finished = (lax.all_gather(both, axis, axis=dim, tiled=True), 0, [])
    for a in arrays:
        finished.append(lax.slice_in_dim(filled, at, at + a.shape[along], axis=along))
        at += a.shape[along]
    return tuple(finished)


def split_up(x, dim, size):
    before, after = (x.shape[:dim], x.shape[dim + 1 :])
    return jnp.moveaxis(x.reshape(*before, size, -1, *after), dim, 0)


def sent_and_summed(x, axis, dim):
    size = lax.axis_size(axis)
    pieces = lax.all_to_all(split_up(x, dim, size), axis, 0, 0, tiled=True)
    return jnp.sum(pieces, axis=0)


def fold_rows(normed, pieces):
    return tuple((jnp.dot(normed, piece, preferred_element_type=jnp.float32) for piece in pieces))


def stored_floats(sums):
    rounded = lax.optimization_barrier(tuple((item.astype(jnp.bfloat16) for item in sums)))
    return tuple((item.astype(jnp.float32) for item in rounded))


def combine_states(earlier, later):
    first = jnp.einsum("hij,hjk->hik", later[0], earlier[0], precision=exact_setting)
    second = jnp.einsum("hij,hjk->hik", later[0], earlier[1], precision=exact_setting) + later[1]
    return (first, second)


def block_product(left, right):
    return jnp.einsum("nhij,nhjk->nhik", left, right, precision=exact_setting)


def pairwise(left, right):
    return jnp.einsum("nhtk,nhik->nhti", left, right, precision=exact_setting)


def scan_mixer(sums, key_gain, removal_gain, removal_bias, decay_bias, decay_extra, scan_norm_gain):
    recept, key_rows, value_rows, decay_pre, removal_pre, gate_pre = stored_floats(sums)
    length = recept.shape[0]
    head_count = recept.shape[1] // HEAD_SIZE
    block_count = length // BLOCK
    decay_rate = jnp.exp(-jax.nn.softplus(-(decay_bias + decay_pre)) - 0.5) + decay_extra
    removal = jax.nn.sigmoid(removal_bias + removal_pre)
    scaled = (key_rows * key_gain).reshape(length, head_count, HEAD_SIZE)
    unit_keys = (
        scaled * lax.rsqrt(jnp.sum(scaled * scaled, axis=-1, keepdims=True) + 1e-06)
    ).reshape(length, -1)
    written = key_rows * (1.0 + (removal - 1.0) * removal_gain)

    def blocked(table):
        return table.reshape(block_count, BLOCK, head_count, HEAD_SIZE).transpose(0, 2, 1, 3)

    recept_b = blocked(recept)
    written_b = blocked(written)
    values_b = blocked(value_rows)
    rate_b = blocked(decay_rate)
    unit_b = blocked(unit_keys)
    removal_b = blocked(removal)
    falling = -jnp.cumsum(rate_b, axis=2)
    before = falling + rate_b
    middle = falling[:, :, BLOCK // 2 : BLOCK // 2 + 1]
    ending = falling[:, :, BLOCK - 1 :]
    alpha = -unit_b
    beta = unit_b * removal_b
    position = jnp.arange(BLOCK)
    strict = (position[:, None] > position[None, :]).astype(jnp.float32)
    inclusive = (position[:, None] >= position[None, :]).astype(jnp.float32)
    alpha_mid = alpha * jnp.exp(before - middle)
    recept_mid = recept_b * jnp.exp(falling - middle)
    beta_mid = beta * jnp.exp(middle - falling)
    keys_mid = written_b * jnp.exp(middle - falling)
    alpha_beta = pairwise(alpha_mid, beta_mid) * strict
    alpha_keys = pairwise(alpha_mid, keys_mid) * strict
    recept_beta = pairwise(recept_mid, beta_mid) * inclusive
    recept_keys = pairwise(recept_mid, keys_mid) * inclusive
    inverse = jnp.eye(BLOCK, dtype=jnp.float32) + alpha_beta
    power = alpha_beta
    for index in range(BLOCK.bit_length() - 2):
        power = block_product(power, power)
        inverse = inverse + block_product(inverse, power)
    widened = jnp.concatenate([values_b, jnp.zeros_like(values_b)], axis=-1)
    rhs_local = block_product(alpha_keys, widened)
    read_local = block_product(recept_keys, widened)
    start_alpha = alpha * jnp.exp(before)
    start_recept = recept_b * jnp.exp(falling)
    end_beta = beta * jnp.exp(ending - falling)
    end_keys = written_b * jnp.exp(ending - falling)
    end_decay = jnp.exp(ending)[:, :, 0, :]

    def advance(carried_state, inputs):
        (
            starting_alpha,
            starting_receptance,
            solver,
            r_beta,
            r_local,
            right_operand,
            ending_beta,
            ending_key_rows,
            e_decay,
            widen_width,
        ) = inputs
        gathered_rows = (
            jnp.einsum("qfl,qlz->qfz", starting_alpha, carried_state, precision=exact_setting)
            + right_operand
        )
        removed_value = jnp.einsum("hti,hiv->htv", solver, gathered_rows, precision=exact_setting)
        readout = (
            jnp.einsum("qfl,qlz->qfz", starting_receptance, carried_state, precision=exact_setting)
            + jnp.einsum("hti,hiv->htv", r_beta, removed_value, precision=exact_setting)
            + r_local
        )
        carried_state = (
            e_decay[:, :, None] * carried_state
            + jnp.einsum("pzw,pzb->pwb", ending_beta, removed_value, precision=exact_setting)
            + jnp.einsum("pzw,pzb->pwb", ending_key_rows, widen_width, precision=exact_setting)
        )
        return (carried_state, readout)

    identity = jnp.broadcast_to(
        jnp.eye(HEAD_SIZE, dtype=jnp.float32), (head_count, HEAD_SIZE, HEAD_SIZE)
    )
    initial = jnp.concatenate([jnp.zeros_like(identity), identity], axis=-1)
    final, readout_rows = lax.scan(
        advance,
        initial,
        (
            start_alpha,
            start_recept,
            inverse,
            recept_beta,
            read_local,
            rhs_local,
            end_beta,
            end_keys,
            end_decay,
            widened,
        ),
    )
    incoming_state = carried_in(
        (final[:, :, HEAD_SIZE:], final[:, :, :HEAD_SIZE]),
        SP,
        combine_states,
        (identity, jnp.zeros_like(identity)),
    )
    reads = readout_rows[..., :HEAD_SIZE] + jnp.einsum(
        "yqem,qmb->yqeb", readout_rows[..., HEAD_SIZE:], incoming_state[1], precision=exact_setting
    )
    reads = reads.transpose(0, 2, 1, 3).reshape(length, head_count, HEAD_SIZE)
    center = jnp.mean(reads, axis=-1, keepdims=True)
    spread = jnp.mean((reads - center) ** 2, axis=-1, keepdims=True)
    normalized = ((reads - center) * lax.rsqrt(spread + 0.00064)).reshape(length, -1)
    return (normalized * scan_norm_gain * jax.nn.sigmoid(gate_pre)).astype(jnp.bfloat16)


def conv_mixer(sums, conv_kernel, conv_bias, conv_norm_gain):
    value_part, gate_part = stored_floats(sums)
    conv_input = (value_part * jax.nn.sigmoid(gate_part)).astype(jnp.bfloat16)
    length = conv_input.shape[0]
    rim = shifted(conv_input[length - (CONV_K - 1) :], SP, 1)
    padded = jnp.concatenate([rim, conv_input], axis=0).astype(jnp.float32)
    filtered = conv_bias + conv_kernel[0] * padded[0:length]
    for index in range(1, CONV_K):
        filtered = filtered + conv_kernel[index] * padded[index : index + length]
    totals = in_one((jnp.sum(filtered, axis=-1), jnp.sum(filtered * filtered, axis=-1)), "tp")
    channels = filtered.shape[1] * lax.axis_size("tp")
    center = totals[0] / channels
    spread = totals[1] / channels - center * center
    scaled = (filtered - center[:, None]) * lax.rsqrt(spread[:, None] + 1e-05) * conv_norm_gain
    return jax.nn.silu(scaled).astype(jnp.bfloat16)


def shards(
    tokens,
    norm_gain,
    query_weight,
    key_weight,
    value_weight,
    decay_weight,
    removal_weight,
    gate_weight,
    key_gain,
    removal_gain,
    removal_bias,
    decay_bias,
    decay_extra,
    scan_norm_gain,
    conv_value_weight,
    conv_gate_weight,
    conv_kernel,
    conv_bias,
    conv_norm_gain,
    out_scan_weight,
    out_conv_weight,
):
    stacked = jnp.concatenate([out_scan_weight, out_conv_weight], axis=0)
    whole = gather_directly(tokens, "tp", 1)
    floats = whole.astype(jnp.float32)
    normed = (
        floats * lax.rsqrt(jnp.mean(floats * floats, axis=-1, keepdims=True) + 1e-06) * norm_gain
    ).astype(jnp.bfloat16)
    projected = fold_rows(
        normed,
        side_by_side(
            (
                query_weight,
                key_weight,
                value_weight,
                decay_weight,
                removal_weight,
                gate_weight,
                conv_value_weight,
                conv_gate_weight,
            ),
            SP,
            0,
            1,
        ),
    )
    scan_sums = projected[:6]
    conv_sums = projected[6:]
    scan_out = scan_mixer(
        scan_sums, key_gain, removal_gain, removal_bias, decay_bias, decay_extra, scan_norm_gain
    )
    conv_out = conv_mixer(conv_sums, conv_kernel, conv_bias, conv_norm_gain)
    features = jnp.concatenate([scan_out, conv_out], axis=1)
    terms = jnp.dot(
        features,
        lax.all_gather(stacked, SP, axis=1, tiled=True),
        preferred_element_type=jnp.float32,
    )
    summed = sent_and_summed(terms, "tp", 1)
    return summed.astype(jnp.bfloat16)


def solution(mesh):
    torus = Mesh(mesh.devices.reshape(8, 8, 2, mesh.shape["tp"]), ("sp_0", "sp_1", "sp_2", "tp"))
    in_specs = (
        P(SP, "tp"),
        P(),
        P(SP, "tp"),
        P(SP, "tp"),
        P(SP, "tp"),
        P(SP, "tp"),
        P(SP, "tp"),
        P(SP, "tp"),
        P("tp"),
        P("tp"),
        P("tp"),
        P("tp"),
        P(SP, "tp"),
        P("tp"),
        P(SP, "tp"),
        P(SP, "tp"),
        P(None, "tp"),
        P("tp"),
        P("tp"),
        P("tp", SP),
        P("tp", SP),
    )
    out_specs = P(SP, "tp")
    return jax.shard_map(
        shards, mesh=torus, in_specs=in_specs, out_specs=out_specs, check_vma=False
    )
```

profile of v0, /device:TPU:24, one launch (start us, length us, event | category | flops | bytes accessed | tf_op | source)
XLA Modules:
  0.0 233.7 jit_solution(4876056362150712214)
XLA Ops:
  7.2 0.7 constant_dynamic-update-slice_fusion.6
  7.9 0.7 constant_dynamic-update-slice_fusion.5
  8.6 0.7 constant_dynamic-update-slice_fusion.4
  9.3 0.7 constant_dynamic-update-slice_fusion.3
  10.0 0.7 constant_dynamic-update-slice_fusion.2
  10.7 0.7 constant_dynamic-update-slice_fusion.1
  11.4 0.7 constant_dynamic-update-slice_fusion
  12.7 1.9 broadcast_in_dim.27
  14.6 4.4 %all-to-all-start = ((bf16[4,192,512]{2,1,0:T(8,128)(2,1)}), bf16[4,192,512]{2,1,0:T(8,128)(2,1)S(1)}, u32[]{:S(2)}, u32[]{:S(2)}) async-start(bf16[4,192,512]{2,1,0:T(8,128)(2,1)} %broadcast_in_dim.27), calls=%async_computation | async-start | bytes 1572864 | tf_op jit(solution)/shard_map/all_to_all | solution.py:62
  19.0 1.3 pad_maximum_fusion.3
  20.6 1.6 slice_bitcast_fusion.29
  22.1 1.7 slice_bitcast_fusion.30
  23.8 7.5 %all-to-all-done = bf16[4,192,512]{2,1,0:T(8,128)(2,1)S(1)} async-done(((bf16[4,192,512]{2,1,0:T(8,128)(2,1)}), bf16[4,192,512]{2,1,0:T(8,128)(2,1)S(1)}, u32[]{:S(2)}, u32[]{:S(2)}) %all-to-all-start) | async-done | bytes 786464 | tf_op jit(solution)/shard_map/all_to_all | solution.py:62
  32.2 69.2 %all-gather.6.cloned.1.call-done = bf16[2048,1024]{1,0:T(8,128)(2,1)} async-done(((bf16[16,1024]{1,0:T(8,128)(2,1)}), bf16[2048,1024]{1,0:T(8,128)(2,1)}) %all-gather.6.cloned.1.call-update) | async-done | bytes 4194320 | tf_op jit(solution)/shard_map/all_gather | solution.py:92
  101.5 1.4 convolution_convert_fusion.7
  102.9 1.4 convolution_convert_fusion.6
  104.3 2.0 convolution_convert_fusion.5
  106.3 1.4 convolution_convert_fusion.4
  107.7 1.4 convolution_convert_fusion.3
  109.1 1.4 convolution_convert_fusion.2
  114.3 1.4 convolution_convert_fusion.1
  115.7 1.4 convolution_convert_fusion
  117.2 2.1 collective-permute-start
  122.5 8.3 %while.12 = (s32[]{:T(128)}, f32[2,64,128]{2,1,0:T(8,128)S(1)}, f32[6,2,32,128]{3,2,0,1:T(8,128)S(1)}, f32[6,2,64]{2,1,0:T(2,128)S(1)}, f32[6,2,32,64]{3,2,1,0:T...) while((s32[]{:T(128)}, f32[2,64,128]{2,1,0:T(8,128)S(1)}, ...), condition=%wide.region_4.5_spmd, body=%wide.region_3.4_spmd.sunk | while | flops 31531008 | bytes 955549 | solution.py:220
  130.9 3.3 %all-gather = f32[512,64]{1,0:T(8,128)S(1)} all-gather(f32[256,64]{1,0:T(8,128)S(1)} %pad_maximum_fusion), channel_id=2, replica_groups=mesh['sp_0'=8,'sp_1'=8,'sp_2'=2,'tp'=4] {'sp_2'}, dimensions={0}, use_global_device_ids=true | all-gather | bytes 196608 | tf_op jit(solution)/shard_map/all_gather | solution.py:30
  135.1 27.0 %all-gather.1 = f32[2048,64]{1,0:T(8,128)S(1)} all-gather(f32[256,64]{1,0:T(8,128)S(1)} %pad_maximum_fusion.1), channel_id=3, replica_groups=mesh['sp_0'=8,'sp_1'=8,'sp_2'=2,'tp'=4] {'sp_1'}, dimensions={0}, use_global_device_ids=true | all-gather | bytes 589824 | tf_op jit(solution)/shard_map/all_gather | solution.py:30
  166.3 26.7 %all-gather.2 = f32[2048,64]{1,0:T(8,128)S(1)} all-gather(f32[256,64]{1,0:T(8,128)S(1)} %pad_maximum_fusion.2), channel_id=4, replica_groups=mesh['sp_0'=8,'sp_1'=8,'sp_2'=2,'tp'=4] {'sp_0'}, dimensions={0}, use_global_device_ids=true | all-gather | bytes 589824 | tf_op jit(solution)/shard_map/all_gather | solution.py:30
  198.0 4.4 %all-to-all-start.1 = ((f32[4,1,384]{2,1,0:T(1,128)}), f32[4,1,384]{2,1,0:T(1,128)S(1)}, u32[]{:S(2)}, u32[]{:S(2)}) async-start(f32[4,1,384]{2,1,0:T(1,128)} %broadcast_in_dim.28), calls=%async_computation.1 | async-start | bytes 12288 | tf_op jit(solution)/shard_map/all_to_all | solution.py:62
  202.4 5.3 %all-to-all-done.1 = f32[4,1,384]{2,1,0:T(1,128)S(1)} async-done(((f32[4,1,384]{2,1,0:T(1,128)}), f32[4,1,384]{2,1,0:T(1,128)S(1)}, u32[]{:S(2)}, u32[]{:S(2)}) %all-to-all-start.1) | async-done | bytes 6176 | tf_op jit(solution)/shard_map/all_to_all | solution.py:62
  208.0 1.7 fusion.77
  209.9 16.1 %all_to_all.16 = f32[4,192,512]{2,1,0:T(8,128)S(1)} all-to-all(f32[4,192,512]{2,1,0:T(8,128)S(1)} %bitcast.328), channel_id=1, replica_groups=mesh['sp_0'=8,'sp_1'=8,'sp_2'=2,'tp'=4] {'tp'}, dimensions={0} | all-to-all | bytes 3145728 | tf_op jit(solution)/shard_map/all_to_all | solution.py:106
  226.0 0.9 reduce_sum.79
  (233 shorter events, 26.7 us)
Async XLA Ops:
  6.5 94.9 %all-gather.6.cloned.1.call-start = ((), (), s32[]{:S(2)}) async-start(), calls=%async_computation.3 | async-start | bytes 4227072 | tf_op jit(solution)/shard_map/all_gather | solution.py:92
  14.6 16.7 %all-to-all-start = ((bf16[4,192,512]{2,1,0:T(8,128)(2,1)}), bf16[4,192,512]{2,1,0:T(8,128)(2,1)S(1)}, u32[]{:S(2)}, u32[]{:S(2)}) async-start(bf16[4,192,512]{2,1,0:T(8,128)(2,1)} %broadcast_in_dim.27), calls=%async_computation | async-start | bytes 1572864 | tf_op jit(solution)/shard_map/all_to_all | solution.py:62
  19.0 189.0 %all-gather.8.cloned.1.call-start = ((), (), s32[]{:S(2)}) async-start(), calls=%async_computation.4 | async-start | bytes 1056768 | tf_op jit(solution)/shard_map/all_gather | solution.py:325
  32.2 78.4 %copy-start = (f32[192,128]{1,0:T(8,128)S(1)}, f32[192,128]{1,0:T(8,128)}, u32[]{:S(2)}) copy-start(f32[192,128]{1,0:T(8,128)} %param.35) | copy-start | bytes 294916
  32.2 78.4 %copy-start.33 = (f32[128]{0:T(128)S(1)}, f32[128]{0:T(128)}, u32[]{:S(2)}) copy-start(f32[128]{0:T(128)} %param.32) | copy-start | bytes 1540
  32.2 78.4 %copy-start.34 = (f32[128]{0:T(128)S(1)}, f32[128]{0:T(128)}, u32[]{:S(2)}) copy-start(f32[128]{0:T(128)} %param.33) | copy-start | bytes 1540
  32.2 78.4 %copy-start.35 = (f32[128]{0:T(128)S(1)}, f32[128]{0:T(128)}, u32[]{:S(2)}) copy-start(f32[128]{0:T(128)} %param.31) | copy-start | bytes 1540
  32.2 78.4 %copy-start.36 = (f32[128]{0:T(128)S(1)}, f32[128]{0:T(128)}, u32[]{:S(2)}) copy-start(f32[128]{0:T(128)} %param.34) | copy-start | bytes 1540
  117.2 79.3 %collective-permute-start = (bf16[30,128]{1,0:T(8,128)(2,1)S(1)}, bf16[30,128]{1,0:T(8,128)(2,1)S(1)}, u32[]{:S(2)}, u32[]{:S(2)}) collective-permute-start(bf16[30,128]{1,0:T(8,128)(2,1)S(1)} %slice.584), channel_id=1, source_target_pairs={{0,4},{4,8},{8,12},{12,16},{16,20},{20,24},{24,28},{28,32},{32,36}... | collective-permute-start | bytes 23048 | tf_op jit(solution)/shard_map/ppermute | solution.py:57
  166.0 30.5 %copy-start.4 = (f32[128]{0:T(128)S(1)}, f32[128]{0:T(128)}, u32[]{:S(2)}) copy-start(f32[128]{0:T(128)} %get-tuple-element.195) | copy-start | bytes 1540
  166.0 30.5 %copy-start.5 = (f32[128]{0:T(128)S(1)}, f32[128]{0:T(128)}, u32[]{:S(2)}) copy-start(f32[128]{0:T(128)} %get-tuple-element.196) | copy-start | bytes 1540
  166.0 30.5 %copy-start.6 = (f32[128]{0:T(128)S(1)}, f32[128]{0:T(128)}, u32[]{:S(2)}) copy-start(f32[128]{0:T(128)} %get-tuple-element.197) | copy-start | bytes 1540
  166.0 30.5 %copy-start.7 = (f32[128]{0:T(128)S(1)}, f32[128]{0:T(128)}, u32[]{:S(2)}) copy-start(f32[128]{0:T(128)} %get-tuple-element.198) | copy-start | bytes 1540
  166.0 30.5 %copy-start.8 = (f32[128]{0:T(128)S(1)}, f32[128]{0:T(128)}, u32[]{:S(2)}) copy-start(f32[128]{0:T(128)} %get-tuple-element.199) | copy-start | bytes 1540
  166.1 30.5 %copy-start.9 = (f32[128]{0:T(128)S(1)}, f32[128]{0:T(128)}, u32[]{:S(2)}) copy-start(f32[128]{0:T(128)} %get-tuple-element.200) | copy-start | bytes 1540
  166.1 30.5 %copy-start.10 = (f32[128]{0:T(128)S(1)}, f32[128]{0:T(128)}, u32[]{:S(2)}) copy-start(f32[128]{0:T(128)} %get-tuple-element.201) | copy-start | bytes 1540
  166.1 30.5 %copy-start.11 = (f32[128]{0:T(128)S(1)}, f32[128]{0:T(128)}, u32[]{:S(2)}) copy-start(f32[128]{0:T(128)} %get-tuple-element.202) | copy-start | bytes 1540
  166.1 30.5 %copy-start.12 = (f32[128]{0:T(128)S(1)}, f32[128]{0:T(128)}, u32[]{:S(2)}) copy-start(f32[128]{0:T(128)} %get-tuple-element.172) | copy-start | bytes 1540
  166.1 30.5 %copy-start.13 = (f32[128]{0:T(128)S(1)}, f32[128]{0:T(128)}, u32[]{:S(2)}) copy-start(f32[128]{0:T(128)} %get-tuple-element.173) | copy-start | bytes 1540
  166.1 30.5 %copy-start.14 = (f32[128]{0:T(128)S(1)}, f32[128]{0:T(128)}, u32[]{:S(2)}) copy-start(f32[128]{0:T(128)} %get-tuple-element.174) | copy-start | bytes 1540
  166.1 30.5 %copy-start.15 = (f32[128]{0:T(128)S(1)}, f32[128]{0:T(128)}, u32[]{:S(2)}) copy-start(f32[128]{0:T(128)} %get-tuple-element.175) | copy-start | bytes 1540
  166.1 30.5 %copy-start.16 = (f32[128]{0:T(128)S(1)}, f32[128]{0:T(128)}, u32[]{:S(2)}) copy-start(f32[128]{0:T(128)} %get-tuple-element.176) | copy-start | bytes 1540
  166.1 30.5 %copy-start.17 = (f32[128]{0:T(128)S(1)}, f32[128]{0:T(128)}, u32[]{:S(2)}) copy-start(f32[128]{0:T(128)} %get-tuple-element.177) | copy-start | bytes 1540
  166.1 30.5 %copy-start.18 = (f32[128]{0:T(128)S(1)}, f32[128]{0:T(128)}, u32[]{:S(2)}) copy-start(f32[128]{0:T(128)} %get-tuple-element.178) | copy-start | bytes 1540
  166.2 30.5 %copy-start.19 = (f32[128]{0:T(128)S(1)}, f32[128]{0:T(128)}, u32[]{:S(2)}) copy-start(f32[128]{0:T(128)} %get-tuple-element.179) | copy-start | bytes 1540
  166.2 30.5 %copy-start.20 = (f32[128]{0:T(128)S(1)}, f32[128]{0:T(128)}, u32[]{:S(2)}) copy-start(f32[128]{0:T(128)} %get-tuple-element.180) | copy-start | bytes 1540
  166.2 30.5 %copy-start.21 = (f32[128]{0:T(128)S(1)}, f32[128]{0:T(128)}, u32[]{:S(2)}) copy-start(f32[128]{0:T(128)} %get-tuple-element.181) | copy-start | bytes 1540
  166.2 30.5 %copy-start.22 = (f32[128]{0:T(128)S(1)}, f32[128]{0:T(128)}, u32[]{:S(2)}) copy-start(f32[128]{0:T(128)} %get-tuple-element.182) | copy-start | bytes 1540
  166.2 30.5 %copy-start.23 = (f32[128]{0:T(128)S(1)}, f32[128]{0:T(128)}, u32[]{:S(2)}) copy-start(f32[128]{0:T(128)} %get-tuple-element.183) | copy-start | bytes 1540
  166.2 30.5 %copy-start.24 = (f32[128]{0:T(128)S(1)}, f32[128]{0:T(128)}, u32[]{:S(2)}) copy-start(f32[128]{0:T(128)} %get-tuple-element.184) | copy-start | bytes 1540
  166.2 30.5 %copy-start.25 = (f32[128]{0:T(128)S(1)}, f32[128]{0:T(128)}, u32[]{:S(2)}) copy-start(f32[128]{0:T(128)} %get-tuple-element.185) | copy-start | bytes 1540
  198.0 9.7 %all-to-all-start.1 = ((f32[4,1,384]{2,1,0:T(1,128)}), f32[4,1,384]{2,1,0:T(1,128)S(1)}, u32[]{:S(2)}, u32[]{:S(2)}) async-start(f32[4,1,384]{2,1,0:T(1,128)} %broadcast_in_dim.28), calls=%async_computation.1 | async-start | bytes 12288 | tf_op jit(solution)/shard_map/all_to_all | solution.py:62
  (11 other events, 231.8 us)
Sparse Core Ops, SparseCore 0:
  12.8 88.5 all-gather.5
  104.5 75.6 all-gather.7
where the time goes:
time: 235 us; the launch traced here: 234 us
  waiting for transfers between devices  82.1 us (35%)
  blocking collectives  73.1 us (31%)
  matrix products  33.3 us (14%)
  between operations  14.8 us (6%)
  local copies, waits for them, and re-layouts  14.6 us (6%)
  starting transfers between devices  10.9 us (5%)
  other arithmetic  4.55 us (2%)
    all_gather x1, waiting for transfers between devices, side_by_side(): lax.all_gather(both, axis, axis=dim, tiled=True)  69.2 us
    all_gather x3, blocking collectives, collected_together(): both, at, found = (lax.all_gather(jnp.concatenate(lines), axis), 0, {})  57 us
    all_to_all x1, blocking collectives, sent_and_summed(): pieces = lax.all_to_all(split_up(x, dim, size), axis, 0, 0, tiled=True)  16.1 us
    all_to_all x2, waiting for transfers between devices, copy_for_each(): lax.all_to_all(jnp.broadcast_to(x[None], (size, *x.shape)), axis, 0, 0, t...  12.8 us
    dot_general x8, matrix products, fold_rows(): jnp.dot(normed, piece, preferred_element_type=jnp.float32)  11.9 us
    all_to_all x2, starting transfers between devices, copy_for_each(): lax.all_to_all(jnp.broadcast_to(x[None], (size, *x.shape)), axis, 0, 0, t...  8.81 us
    unnamed x83, local copies, waits for them, and re-layouts  5.63 us
  transfers between devices with their start and end apart: 5, of which 3 were waited for; matrix products, arithmetic and copies ran while one was open for 19% of the time, Pallas kernels for 0%

commit v1 on v0

v1 whole, which is shorter than its diff:
```python
import functools
import math

import jax
import jax.numpy as jnp
from jax import lax
from jax.experimental import pallas as pl
from jax.experimental.pallas import tpu as pltpu
from jax.sharding import Mesh
from jax.sharding import PartitionSpec as P

F32 = jnp.float32
BF16 = jnp.bfloat16
SP = ("sp_0", "sp_1", "sp_2")
MESH = pl.DeviceIdType.MESH
CONV_K = 31
ROWS = 192
BLOCK = 64
BLOCKS = ROWS // BLOCK
MODEL = 2048
NX = 4
PROJ = 1024
CHUNK = 1280
N = 8


def split2(a):
    high = a.astype(BF16)
    return high, (a - high.astype(F32)).astype(BF16)


def one(a, b):
    return jnp.dot(a.astype(BF16), b.astype(BF16), preferred_element_type=F32)


def one_nt(a, b):
    return lax.dot_general(
        a.astype(BF16), b.astype(BF16), (((1,), (1,)), ((), ())), preferred_element_type=F32
    )


def three(a, b):
    ah, al = split2(a)
    bh, bl = split2(b)
    return one(ah, bh) + one(al, bh) + one(ah, bl)


def three_nt(a, b):
    ah, al = split2(a)
    bh, bl = split2(b)
    return one_nt(ah, bh) + one_nt(al, bh) + one_nt(ah, bl)


def left_exact(a, b):
    bh, bm = split2(b)
    bl = (b - bh.astype(F32) - bm.astype(F32)).astype(BF16)
    return one(a, bh) + one(a, bm) + one(a, bl)


def right_exact(a, b):
    ah, al = split2(a)
    return one(ah, b) + one(al, b)


def iotas(rows, columns):
    return (
        lax.broadcasted_iota(jnp.int32, (rows, columns), 0),
        lax.broadcasted_iota(jnp.int32, (rows, columns), 1),
    )


def sigmoid(x):
    return 1.0 / (1.0 + jnp.exp(-x))


def head_ones():
    i, j = iotas(128, 128)
    return ((i >> 6) == (j >> 6)).astype(BF16)


def local_scan(
    recept, keys, values, decay_pre, removal_pre, key_gain, removal_gain, removal_bias, decay_bias, extra
):
    ones = head_ones()
    rate = sigmoid(decay_bias + decay_pre) * math.exp(-0.5) + extra
    removal = sigmoid(removal_bias + removal_pre)
    scaled = keys * key_gain
    unit = scaled * lax.rsqrt(right_exact(scaled * scaled, ones) + 1e-06)
    written = keys * (1.0 + (removal - 1.0) * removal_gain)
    beta = unit * removal
    i, j = iotas(BLOCK, BLOCK)
    lower = (i >= j).astype(BF16)

    lane = lax.broadcasted_iota(jnp.int32, (BLOCK, 128), 1)
    first = lane < 64

    def spread(a):
        return jnp.concatenate([jnp.where(first, a, 0.0), jnp.where(first, 0.0, a)], axis=0)

    i, j = iotas(128, 128)
    same_head = (i >> 6) == (j >> 6)
    inclusive = same_head & (i >= j)
    strict = same_head & (i > j)
    eye = (i == j).astype(F32)
    sames = [(i >> s) == (j >> s) for s in (3, 4, 5)] + [same_head]

    parts = []
    for b in range(BLOCKS):
        rows = slice(b * BLOCK, (b + 1) * BLOCK)
        rate_b = rate[rows]
        falling = -left_exact(lower, rate_b)
        before = falling + rate_b
        middle = falling[BLOCK // 2 : BLOCK // 2 + 1]
        ending = falling[BLOCK - 1 :]
        up = jnp.exp(middle - falling)
        alpha_mid = -unit[rows] * jnp.exp(before - middle)
        recept_mid = recept[rows] * jnp.exp(falling - middle)
        beta_mid = beta[rows] * up
        keys_mid = written[rows] * up
        to_end = jnp.exp(ending - falling)
        end_decay = jnp.exp(ending)
        start_alpha = spread(-unit[rows] * jnp.exp(before))
        start_recept = spread(recept[rows] * jnp.exp(falling))
        end_beta = spread(beta[rows] * to_end)
        end_keys = spread(written[rows] * to_end)
        values_b = spread(values[rows])
        left = jnp.concatenate([spread(alpha_mid), spread(recept_mid)], axis=0)
        right = jnp.concatenate([beta_mid, beta_mid, keys_mid, keys_mid], axis=0)
        pairs = three_nt(left, right)
        alpha_beta = jnp.where(strict, pairs[:128, :128], 0.0)
        alpha_keys = jnp.where(strict, pairs[:128, 128:], 0.0)
        recept_beta = jnp.where(inclusive, pairs[128:, :128], 0.0)
        recept_keys = jnp.where(inclusive, pairs[128:, 128:], 0.0)
        local = three(jnp.concatenate([alpha_keys, recept_keys], axis=0), values_b)
        base = jnp.where(sames[0], alpha_beta, 0.0)
        inverse = eye + base
        power = three(base, base)
        inverse = inverse + three(inverse, power)
        power = three(power, power)
        inverse = inverse + three(inverse, power)
        for s in range(3):
            off = jnp.where(sames[s + 1] & ~sames[s], alpha_beta, 0.0)
            inverse = inverse + three(inverse, three(off, inverse))
        gathered = three(inverse, jnp.concatenate([start_alpha, local[:128]], axis=1))
        step = three(end_beta.T, gathered)
        step_a = step[:, :128] + jnp.where(i == j, end_decay, 0.0)
        step_b = step[:, 128:] + three(end_keys.T, values_b)
        reads = three(recept_beta, gathered)
        read_a = reads[:, :128] + start_recept
        read_b = reads[:, 128:] + local[128:]
        parts.append(
            (step_a, step_b, read_a[:64] + read_a[64:], read_b[:64] + read_b[64:])
        )
    trans_a, trans_b = parts[0][0], parts[0][1]
    reads_a, reads_b = [parts[0][2]], [parts[0][3]]
    for b in range(1, BLOCKS):
        step_a, step_b, read_a, read_b = parts[b]
        both = jnp.concatenate([trans_a, trans_b], axis=1)
        seen = three(read_a, both)
        reads_a.append(seen[:, :128])
        reads_b.append(seen[:, 128:] + read_b)
        moved = three(step_a, both)
        trans_a, trans_b = moved[:, :128], moved[:, 128:] + step_b
    return (
        trans_a,
        trans_b,
        jnp.concatenate(reads_a, axis=0),
        jnp.concatenate(reads_b, axis=0),
    )


def packed_heads(trans_a, trans_b):
    lane = lax.broadcasted_iota(jnp.int32, (64, 128), 1)
    head0 = jnp.where(lane < 64, trans_a[:64], pltpu.roll(trans_b[:64], 64, 1))
    head1 = jnp.where(lane < 64, pltpu.roll(trans_a[64:], 64, 1), trans_b[64:])
    return head0, head1


def combine(later, total):
    lane = lax.broadcasted_iota(jnp.int32, later.shape, 1)
    return three(later[:, :64], total) + jnp.where(lane < 64, 0.0, later)


def kernel(
    tokens,
    norm_gain,
    w0,
    w1,
    w2,
    w3,
    w4,
    w5,
    w6,
    w7,
    out_scan,
    out_conv,
    key_gain,
    removal_gain,
    removal_bias,
    decay_bias,
    extra,
    scan_norm_gain,
    conv_kernel,
    conv_bias,
    conv_norm_gain,
    out,
    weights,
    tok,
    normed,
    proj,
    outw,
    pair_in,
    line_y,
    line_z,
    state_in,
    state_out,
    pair_out,
    rim,
    conv_in,
    conv_pad,
    stats,
    feats_scan,
    feats_conv,
    reads_a,
    reads_b,
    mine,
    load_sem,
    tok_send,
    tok_recv,
    first_send,
    first_recv,
    second_send,
    plus_recv,
    minus_recv,
    cross_send,
    cross_recv,
    outw_send,
    outw_recv,
    outw_load,
    pair_send,
    pair_recv,
    y_send,
    y_recv,
    z_send,
    z_recv,
    state_send,
    state_recv,
    rim_send,
    rim_recv,
    stats_send,
    stats_recv,
    scan_send,
    scan_recv,
    conv_send,
    conv_recv,
):
    z, y, c, x = (lax.axis_index(n) for n in (*SP, "tp"))

    def at(z_=None, y_=None, c_=None, x_=None):
        pick = lambda a, b: a if b is None else b
        return (pick(z, z_), pick(y, y_), pick(c, c_), pick(x, x_))

    def remote(src, dst, send, recv, where):
        return pltpu.make_async_remote_copy(
            src_ref=src, dst_ref=dst, send_sem=send, recv_sem=recv, device_id=where, device_id_type=MESH
        )

    partner = at(c_=1 - c)

    loads = [
        pltpu.make_async_copy(tokens, tok.at[x], load_sem.at[0]),
    ]
    for k, w in enumerate((w0, w1, w2, w3, w4, w5, w6, w7)):
        loads.append(
            pltpu.make_async_copy(
                w, weights.at[z, y, c, :, pl.ds(128 * k, 128)], load_sem.at[k + 1]
            )
        )
    for load in loads:
        load.start()
    weights[z, y, c, :, pl.ds(1024, 128)] = out_scan[...].astype(F32).T.astype(BF16)
    weights[z, y, c, :, pl.ds(1152, 128)] = out_conv[...].astype(F32).T.astype(BF16)

    barrier = pltpu.get_barrier_semaphore()
    greeted = [partner]
    for k in range(1, N):
        greeted.append(at(y_=lax.rem(y + k, N)))
        greeted.append(at(z_=lax.rem(z + k, N)))
    for k in range(1, NX):
        greeted.append(at(x_=lax.rem(x + k, NX)))
    place = (z * N + y) * 2 + c
    size = 2 * N * N
    before = lax.rem(place + size - 1, size)
    after = lax.rem(place + 1, size)
    as_device = lambda s: (s // (2 * N), lax.rem(s // 2, N), lax.rem(s, 2), x)
    greeted.append(as_device(before))
    for device in greeted:
        pl.semaphore_signal(barrier, inc=1, device_id=device, device_id_type=MESH)
    pl.semaphore_wait(barrier, len(greeted))
    for load in loads:
        load.wait()

    tok_copies = []
    for k in (1, 3, 2):
        tok_copies.append(
            remote(tok.at[x], tok.at[x], tok_send.at[k - 1], tok_recv.at[k - 1], at(x_=lax.rem(x + k, NX)))
        )
    a = (1 - c) * y + c * z
    b = (1 - c) * z + c * y

    def along_first(k):
        return at(z_=lax.rem(z + c * k, N), y_=lax.rem(y + (1 - c) * k, N))

    def along_second(k):
        return at(z_=lax.rem(z + (1 - c) * k, N), y_=lax.rem(y + c * k, N))

    def slot(from_first, from_second):
        a_ = lax.rem(a + N - from_first, N)
        b_ = lax.rem(b + N - from_second, N)
        z_ = (1 - c) * b_ + c * a_
        y_ = (1 - c) * a_ + c * b_
        return weights.at[z_, y_, c]

    own = slot(0, 0)
    order = (1, 7, 2, 6, 3, 5, 4)
    for k in order:
        remote(own, own, first_send, first_recv.at[k - 1], along_first(k)).start()
    for copy in tok_copies:
        copy.start()

    def push(k, d, sign, ref):
        recv = (plus_recv if sign > 0 else minus_recv).at[k * 4 + d]
        remote(ref, ref, second_send, recv, along_second(1 if sign > 0 else N - 1)).start()

    def arrived(k, d, sign):
        ref = slot(k, d if sign > 0 else N - d)
        if d == 0:
            if k:
                remote(ref, ref, first_send, first_recv.at[k - 1], along_first(k)).wait_recv()
            push(k, 0, 1, ref)
            push(k, 0, -1, ref)
        else:
            recv = (plus_recv if sign > 0 else minus_recv).at[k * 4 + d - 1]
            remote(ref, ref, second_send, recv, partner).wait_recv()
            if d < 3 or (d == 3 and (k % 2 == 0) == (sign > 0)):
                push(k, d, sign, ref)
        remote(ref, ref, cross_send, cross_recv, partner).start()

    events = []
    for k in range(N):
        near = min(k, N - k)
        events.append((near, 0, k, 1))
        for d in range(1, 5):
            for sign in (1, -1):
                if d < 4 or (k % 2 == 0) == (sign > 0):
                    events.append((near + d, d, k, sign))
    events.sort()

    normed_at = len(events) * 5 // 8
    for number, (_, d, k, sign) in enumerate(events):
        arrived(k, d, sign)
        if number == normed_at:
            for copy in tok_copies:
                copy.wait_recv()
            square = jnp.zeros((ROWS, 1), F32)
            for q in range(NX):
                t = tok[q].astype(F32)
                square = square + jnp.sum(t * t, axis=-1, keepdims=True)
            factor = lax.rsqrt(square * (1.0 / MODEL) + 1e-06)
            for q in range(NX):
                t = tok[q].astype(F32)
                columns = slice(q * 512, (q + 1) * 512)
                normed[:, columns] = (t * factor * norm_gain[:, columns]).astype(BF16)

    everything = weights.at[:, :, 1 - c]
    remote(everything, everything, cross_send, cross_recv, partner).wait_recv()

    outw_copies = []
    for k in (1, 3, 2):
        x_ = lax.rem(x + k, NX)
        outw_copies.append(
            remote(
                weights.at[pl.ds(2 * x_, 2), :, :, :, pl.ds(1024, 256)],
                outw.at[x],
                outw_send.at[k - 1],
                outw_recv.at[k - 1],
                at(x_=x_),
            )
        )
    for copy in outw_copies:
        copy.start()
    outw_own = pltpu.make_async_copy(
        weights.at[pl.ds(2 * x, 2), :, :, :, pl.ds(1024, 256)], outw.at[x], outw_load
    )
    outw_own.start()

    def project(n, carry):
        columns = pl.ds(pl.multiple_of(n * 256, 256), 256)
        w = weights[:, :, :, :, columns].reshape(MODEL, 256)
        proj[:, columns] = jnp.dot(normed[...], w, preferred_element_type=F32).astype(BF16)
        return carry

    lax.fori_loop(0, PROJ // 256, project, 0)

    def part(k):
        return proj[:, 128 * k : 128 * (k + 1)].astype(F32)

    conv_in[...] = (part(6) * sigmoid(part(7))).astype(BF16)
    last = place == size - 1
    start = place == 0
    rim_copy = remote(
        conv_in.at[pl.ds(ROWS - 32, 32)], rim, rim_send, rim_recv, as_device(after)
    )

    @pl.when(jnp.logical_not(last))
    def _():
        rim_copy.start()

    trans_a, trans_b, ra, rb = local_scan(
        part(0),
        part(1),
        part(2),
        part(3),
        part(4),
        key_gain[...],
        removal_gain[...],
        removal_bias[...],
        decay_bias[...],
        extra[...],
    )
    reads_a[...] = ra
    reads_b[...] = rb
    head0, head1 = packed_heads(trans_a, trans_b)
    upper = c == 1
    pair_out[...] = jnp.where(upper, head0, head1)
    mine[...] = jnp.where(upper, head1, head0)
    pair_copy = remote(pair_out, pair_in, pair_send, pair_recv, partner)
    pair_copy.start()
    pair_copy.wait_recv()
    earlier = jnp.where(upper, pair_in[...], mine[...])
    later = jnp.where(upper, mine[...], pair_in[...])
    line_y[y] = combine(later, earlier)
    for k in (4, 3, 5, 2, 6, 1, 7):
        remote(line_y.at[y], line_y.at[y], y_send, y_recv.at[y], at(y_=lax.rem(y + k, N))).start()

    @pl.when(start)
    def _():
        rim[...] = jnp.zeros_like(rim)

    @pl.when(jnp.logical_not(start))
    def _():
        rim_copy.wait_recv()

    conv_pad[pl.ds(0, 32)] = rim[...].astype(F32)
    conv_pad[pl.ds(32, ROWS)] = conv_in[...].astype(F32)
    filtered = conv_bias[...] + conv_kernel[0:1] * conv_pad[pl.ds(2, ROWS)]
    for k in range(1, CONV_K):
        filtered = filtered + conv_kernel[k : k + 1] * conv_pad[pl.ds(2 + k, ROWS)]
    near = jnp.mean(filtered, axis=-1, keepdims=True)
    around = jnp.sum((filtered - near) ** 2, axis=-1, keepdims=True)
    lane = lax.broadcasted_iota(jnp.int32, (ROWS, 128), 1)
    stats[x] = jnp.where(lane < 64, near, around)
    conv_pad[pl.ds(0, ROWS)] = filtered
    stats_copies = [
        remote(stats.at[x], stats.at[x], stats_send.at[k - 1], stats_recv.at[k - 1], at(x_=lax.rem(x + k, NX)))
        for k in (1, 3, 2)
    ]
    for copy in stats_copies:
        copy.start()

    lane = lax.broadcasted_iota(jnp.int32, (64, 128), 1)
    i, j = iotas(64, 128)
    blank = (i == j).astype(F32)
    total = inside = blank
    for k in range(N):

        @pl.when(y != k)
        def _():
            remote(line_y.at[k], line_y.at[k], y_send, y_recv.at[k], partner).wait_recv()

        total = combine(line_y[k], total)
        inside = jnp.where(k < y, total, inside)
    line_z[z] = total
    z_copies = []
    for k in range(N - 1, 0, -1):
        copy = remote(
            line_z.at[z], line_z.at[z], z_send.at[k - 1], z_recv.at[z], at(z_=lax.rem(z + k, N))
        )
        z_copies.append((k, copy))

        @pl.when(z + k < N)
        def _():
            copy.start()

    for copy in stats_copies:
        copy.wait_recv()
    center = jnp.zeros((ROWS, 1), F32)
    for q in range(NX):
        center = center + stats[q][:, 0:1]
    center = center * (1.0 / NX)
    spread = jnp.zeros((ROWS, 1), F32)
    for q in range(NX):
        gap = stats[q][:, 0:1] - center
        spread = spread + stats[q][:, 64:65] + 128.0 * gap * gap
    spread = spread * (1.0 / 512.0)
    normal = (conv_pad[pl.ds(0, ROWS)] - center) * lax.rsqrt(spread + 1e-05) * conv_norm_gain[...]
    feats_conv[x] = (normal * sigmoid(normal)).astype(BF16)
    conv_copies = [
        remote(
            feats_conv.at[x], feats_conv.at[x], conv_send.at[k - 1], conv_recv.at[k - 1], at(x_=lax.rem(x + k, NX))
        )
        for k in (1, 3, 2)
    ]
    for copy in conv_copies:
        copy.start()

    def advance(k, state):
        remote(line_z.at[k], line_z.at[k], z_send.at[0], z_recv.at[k], partner).wait_recv()
        return combine(line_z[k], state)

    state = lax.fori_loop(0, z, advance, jnp.zeros((64, 128), F32))
    state = jnp.where(lane < 64, 0.0, combine(inside, state))
    passed = combine(jnp.where(upper, pair_in[...], mine[...]), state)
    here = jnp.where(upper, passed, state)
    state_out[...] = jnp.where(upper, state, passed)
    state_copy = remote(state_out, state_in, state_send, state_recv, partner)
    state_copy.start()

    for copy in conv_copies:
        copy.wait_recv()
    for copy in outw_copies:
        copy.wait_recv()
    outw_own.wait()
    w_of = lambda q, h: outw[q, :, :, :, :, pl.ds(128 * h, 128)].reshape(512, 128)
    total_out = one_nt(feats_conv[0], w_of(0, 1))
    for q in range(1, NX):
        total_out = total_out + one_nt(feats_conv[q], w_of(q, 1))

    state_copy.wait_recv()
    there = state_in[...]
    state0 = jnp.where(upper, there, here)
    state1 = jnp.where(upper, here, there)
    whole = jnp.concatenate(
        [
            jnp.where(lane < 64, pltpu.roll(state0, 64, 1), 0.0),
            jnp.where(lane < 64, 0.0, state1),
        ],
        axis=0,
    )
    reads = three(reads_a[...], whole) + reads_b[...]
    ones = head_ones()
    reads = reads - right_exact(reads, ones) * (1.0 / 64.0)
    spread = right_exact(reads * reads, ones) * (1.0 / 64.0)
    feats_scan[x] = (
        reads * lax.rsqrt(spread + 0.00064) * scan_norm_gain[...] * sigmoid(part(5))
    ).astype(BF16)
    scan_copies = [
        remote(
            feats_scan.at[x], feats_scan.at[x], scan_send.at[k - 1], scan_recv.at[k - 1], at(x_=lax.rem(x + k, NX))
        )
        for k in (1, 3, 2)
    ]
    for copy in scan_copies:
        copy.start()
    for copy in scan_copies:
        copy.wait_recv()
    for q in range(NX):
        total_out = total_out + one_nt(feats_scan[q], w_of(q, 0))
    out[...] = total_out.astype(BF16)

    for copies in (tok_copies, outw_copies, stats_copies, conv_copies, scan_copies):
        for copy in copies:
            copy.wait_send()
    pair_copy.wait_send()
    state_copy.wait_send()
    seven = weights.at[pl.ds(0, 7), 0, 0]
    remote(seven, seven, first_send, first_recv.at[0], partner).wait_send()
    most = weights.at[pl.ds(0, 7), :, 0]
    remote(most, most, second_send, plus_recv.at[0], partner).wait_send()
    remote(everything, everything, cross_send, cross_recv, partner).wait_send()
    lines = line_y.at[pl.ds(0, 7)]
    remote(lines, lines, y_send, y_recv.at[0], partner).wait_send()

    @pl.when(jnp.logical_not(last))
    def _():
        rim_copy.wait_send()

    for k, copy in z_copies:

        @pl.when(z + k < N)
        def _():
            copy.wait_send()


def shards(
    tokens,
    norm_gain,
    query_weight,
    key_weight,
    value_weight,
    decay_weight,
    removal_weight,
    gate_weight,
    key_gain,
    removal_gain,
    removal_bias,
    decay_bias,
    decay_extra,
    scan_norm_gain,
    conv_value_weight,
    conv_gate_weight,
    conv_kernel,
    conv_bias,
    conv_norm_gain,
    out_scan_weight,
    out_conv_weight,
):
    row = lambda v: v.reshape(1, -1)
    anywhere = pl.BlockSpec(memory_space=pl.ANY)
    inside = pl.BlockSpec(memory_space=pltpu.VMEM)
    dma = pltpu.SemaphoreType.DMA
    return pl.pallas_call(
        kernel,
        out_shape=jax.ShapeDtypeStruct((ROWS, 512), BF16),
        in_specs=[anywhere] + [inside] + [anywhere] * 8 + [inside] * 11,
        out_specs=inside,
        scratch_shapes=[
            pltpu.VMEM((N, N, 2, 16, CHUNK), BF16),
            pltpu.VMEM((NX, ROWS, 512), BF16),
            pltpu.VMEM((ROWS, MODEL), BF16),
            pltpu.VMEM((ROWS, PROJ), BF16),
            pltpu.VMEM((NX, 2, N, 2, 16, 256), BF16),
            pltpu.VMEM((64, 128), F32),
            pltpu.VMEM((N, 64, 128), F32),
            pltpu.VMEM((N, 64, 128), F32),
            pltpu.VMEM((64, 128), F32),
            pltpu.VMEM((64, 128), F32),
            pltpu.VMEM((64, 128), F32),
            pltpu.VMEM((32, 128), BF16),
            pltpu.VMEM((ROWS, 128), BF16),
            pltpu.VMEM((ROWS + 32, 128), F32),
            pltpu.VMEM((NX, ROWS, 128), F32),
            pltpu.VMEM((NX, ROWS, 128), BF16),
            pltpu.VMEM((NX, ROWS, 128), BF16),
            pltpu.VMEM((ROWS, 128), F32),
            pltpu.VMEM((ROWS, 128), F32),
            pltpu.VMEM((64, 128), F32),
            dma((9,)),
            dma((3,)),
            dma((3,)),
            dma(()),
            dma((7,)),
            dma(()),
            dma((32,)),
            dma((32,)),
            dma(()),
            dma(()),
            dma((3,)),
            dma((3,)),
            dma(()),
            dma(()),
            dma(()),
            dma(()),
            dma((N,)),
            dma((N - 1,)),
            dma((N,)),
            dma(()),
            dma(()),
            dma(()),
            dma(()),
            dma((3,)),
            dma((3,)),
            dma((3,)),
            dma((3,)),
            dma((3,)),
            dma((3,)),
        ],
        compiler_params=pltpu.CompilerParams(
            collective_id=0, has_side_effects=True, vmem_limit_bytes=56 * 1024 * 1024
        ),
    )(
        tokens,
        row(norm_gain),
        query_weight,
        key_weight,
        value_weight,
        decay_weight,
        removal_weight,
        gate_weight,
        conv_value_weight,
        conv_gate_weight,
        out_scan_weight,
        out_conv_weight,
        row(key_gain),
        row(removal_gain),
        row(removal_bias),
        row(decay_bias),
        decay_extra,
        row(scan_norm_gain),
        conv_kernel,
        row(conv_bias),
        row(conv_norm_gain),
    )


def solution(mesh):
    torus = Mesh(mesh.devices.reshape(N, N, 2, mesh.shape["tp"]), (*SP, "tp"))
    in_specs = (
        P(SP, "tp"),
        P(),
        P(SP, "tp"),
        P(SP, "tp"),
        P(SP, "tp"),
        P(SP, "tp"),
        P(SP, "tp"),
        P(SP, "tp"),
        P("tp"),
        P("tp"),
        P("tp"),
        P("tp"),
        P(SP, "tp"),
        P("tp"),
        P(SP, "tp"),
        P(SP, "tp"),
        P(None, "tp"),
        P("tp"),
        P("tp"),
        P("tp", SP),
        P("tp", SP),
    )
    return jax.shard_map(
        shards, mesh=torus, in_specs=in_specs, out_specs=P(SP, "tp"), check_vma=False
    )
```

time: 235 us -> 76.1 us (0.32)
  the two profiles are of different devices: /device:TPU:24 before, /device:TPU:129 now
where the time goes in v1:
time: 76.1 us; the launch traced here: 75.9 us
  Pallas kernels  72.1 us (95%)
  local copies, waits for them, and re-layouts  3.74 us (5%)
    pallas_call x1, Pallas kernels, shards(): pl.pallas_call(kernel, out_shape=jax.ShapeDtypeStruct((ROWS, 512), BF16),...  72.1 us
    unnamed x7, local copies, waits for them, and re-layouts  3.74 us

profile of v1, /device:TPU:129, one launch (start us, length us, event | category | flops | bytes accessed | tf_op | source)
XLA Modules:
  0.0 75.9 jit_solution(5233930776887031488)
XLA Ops:
  0.0 0.0 copy-start
  0.0 0.7 copy-done
  0.7 0.0 copy-start.1
  0.7 0.7 copy.22.out_scan
  1.4 0.0 copy-done.1
  1.4 0.7 copy.23.out_conv
  2.1 72.1 %shard_map.199 = bf16[192,512]{1,0:T(8,128)(2,1)} custom-call(bf16[192,512]{1,0:T(8,128)(2,1)} %tokens.1, f32[1,2048]{1,0:T(1,128)} %bitcast.8, bf16[16,128]{1,0:T(8,128)(2,1)} %w0.1, bf16[16,128]{1,0:T(8,128)(2,1)} %w1.1, bf16[16,128]{1,0:T(8,128)(2,1)} %w2.1, bf16[16,128]{1,0:T(8,128)(2,1)} %w3.1, bf16[16,128]{1,0:T(8,128)(2,1)} %w4.1, ...), custom_call_target="tpu_custom_call" | custom-call | tf_op jit(solution)/shard_map/pallas_call | solution.py:622
  74.3 1.6 %copy.25 = bf16[192,512]{1,0:T(8,128)(2,1)} copy(bf16[192,512]{1,0:T(8,128)(2,1)} %shard_map.199) | data formatting | bytes 393216
Async XLA Ops:
  0.0 0.7 copy-start
  0.7 0.7 copy-start.1

commit v2 on v1

--- a/solution.py
+++ b/solution.py
@@ -20,7 +20,6 @@
 MODEL = 2048
 NX = 4
 PROJ = 1024
-CHUNK = 1280
 N = 8
 
 
@@ -205,10 +204,15 @@
     conv_norm_gain,
     out,
     weights,
+    outs,
+    extra_v,
+    norm_gain_v,
+    conv_kernel_v,
     tok,
     normed,
     proj,
-    outw,
+    outw0,
+    outw1,
     pair_in,
     line_y,
     line_z,
@@ -234,6 +238,13 @@
     minus_recv,
     cross_send,
     cross_recv,
+    first_send2,
+    first_recv2,
+    second_send2,
+    plus_recv2,
+    minus_recv2,
+    outw_cross_send,
+    outw_cross_recv,
     outw_send,
     outw_recv,
     outw_load,
@@ -267,19 +278,25 @@
 
     partner = at(c_=1 - c)
 
+    a = (1 - c) * y + c * z
+    b = (1 - c) * z + c * y
+
     loads = [
         pltpu.make_async_copy(tokens, tok.at[x], load_sem.at[0]),
     ]
     for k, w in enumerate((w0, w1, w2, w3, w4, w5, w6, w7)):
         loads.append(
-            pltpu.make_async_copy(
-                w, weights.at[z, y, c, :, pl.ds(128 * k, 128)], load_sem.at[k + 1]
-            )
-        )
+            pltpu.make_async_copy(w, weights.at[c, b, a, :, pl.ds(128 * k, 128)], load_sem.at[k + 1])
+        )
+    for k, w in enumerate((out_scan, out_conv)):
+        loads.append(
+            pltpu.make_async_copy(w, outs.at[c, b, a, :, pl.ds(128 * k, 128)], load_sem.at[k + 9])
+        )
+    loads.append(pltpu.make_async_copy(extra, extra_v, load_sem.at[11]))
+    loads.append(pltpu.make_async_copy(norm_gain, norm_gain_v, load_sem.at[12]))
+    loads.append(pltpu.make_async_copy(conv_kernel, conv_kernel_v, load_sem.at[13]))
     for load in loads:
         load.start()
-    weights[z, y, c, :, pl.ds(1024, 128)] = out_scan[...].astype(F32).T.astype(BF16)
-    weights[z, y, c, :, pl.ds(1152, 128)] = out_conv[...].astype(F32).T.astype(BF16)
 
     barrier = pltpu.get_barrier_semaphore()
     greeted = [partner]
@@ -305,61 +322,78 @@
         tok_copies.append(
             remote(tok.at[x], tok.at[x], tok_send.at[k - 1], tok_recv.at[k - 1], at(x_=lax.rem(x + k, NX)))
         )
-    a = (1 - c) * y + c * z
-    b = (1 - c) * z + c * y
-
     def along_first(k):
         return at(z_=lax.rem(z + c * k, N), y_=lax.rem(y + (1 - c) * k, N))
 
     def along_second(k):
         return at(z_=lax.rem(z + (1 - c) * k, N), y_=lax.rem(y + c * k, N))
 
-    def slot(from_first, from_second):
-        a_ = lax.rem(a + N - from_first, N)
-        b_ = lax.rem(b + N - from_second, N)
-        z_ = (1 - c) * b_ + c * a_
-        y_ = (1 - c) * a_ + c * b_
-        return weights.at[z_, y_, c]
-
-    own = slot(0, 0)
-    order = (1, 7, 2, 6, 3, 5, 4)
-    for k in order:
-        remote(own, own, first_send, first_recv.at[k - 1], along_first(k)).start()
+    class Gather:
+        def __init__(self, ref, first_send, first_recv, second_send, plus_recv, minus_recv):
+            self.ref, self.first_send, self.first_recv = ref, first_send, first_recv
+            self.second_send, self.recvs = second_send, {1: plus_recv, -1: minus_recv}
+            self.own_half = (a // 4) * 4
+
+        def start(self):
+            own = self.ref.at[c, b, a]
+            for k in (1, 7, 2, 6, 3, 5, 4):
+                remote(own, own, self.first_send, self.first_recv.at[a], along_first(k)).start()
+
+        def half(self, h, distance):
+            low = self.own_half if h == 0 else 4 - self.own_half
+            return self.ref.at[c, lax.rem(b + distance + N, N), pl.ds(low, 4)]
+
+        def copy(self, h, distance, sign, hop):
+            piece = self.half(h, distance)
+            recv = self.recvs[sign].at[h * 4 + hop]
+            return remote(piece, piece, self.second_send, recv, along_second(1 if sign > 0 else N - 1))
+
+        def collect(self, h):
+            low = self.own_half if h == 0 else 4 - self.own_half
+            for k in range(4):
+                a_ = low + k
+
+                @pl.when(a_ != a)
+                def _():
+                    piece = self.ref.at[c, b, a_]
+                    remote(piece, piece, self.first_send, self.first_recv.at[a_], partner).wait_recv()
+
+            for sign in (1, -1):
+                self.copy(h, 0, sign, 0).start()
+            return self.half(h, 0)
+
+        def moved(self, h, hop, sign):
+            self.copy(h, -sign * hop, sign, hop - 1).wait_recv()
+            if hop < 3 or (hop == 3 and (h == 0) == (sign > 0)):
+                self.copy(h, -sign * hop, sign, hop).start()
+            return self.half(h, -sign * hop)
+
+        def step(self, hop):
+            for h in (0, 1):
+                if hop == 0:
+                    yield self.collect(h)
+                    continue
+                for sign in (1, -1):
+                    if hop < 4 or (h == 0) == (sign > 0):
+                        yield self.moved(h, hop, sign)
+
+        def drain(self):
+            seven = self.ref.at[0, 0, pl.ds(0, 7)]
+            remote(seven, seven, self.first_send, self.first_recv.at[0], partner).wait_send()
+            most = self.ref.at[0, pl.ds(0, 7)]
+            remote(most, most, self.second_send, self.first_recv.at[0], partner).wait_send()
+
+    wide = Gather(weights, first_send, first_recv, second_send, plus_recv, minus_recv)
+    thin = Gather(outs, first_send2, first_recv2, second_send2, plus_recv2, minus_recv2)
+    wide.start()
     for copy in tok_copies:
         copy.start()
-
-    def push(k, d, sign, ref):
-        recv = (plus_recv if sign > 0 else minus_recv).at[k * 4 + d]
-        remote(ref, ref, second_send, recv, along_second(1 if sign > 0 else N - 1)).start()
-
-    def arrived(k, d, sign):
-        ref = slot(k, d if sign > 0 else N - d)
-        if d == 0:
-            if k:
-                remote(ref, ref, first_send, first_recv.at[k - 1], along_first(k)).wait_recv()
-            push(k, 0, 1, ref)
-            push(k, 0, -1, ref)
-        else:
-            recv = (plus_recv if sign > 0 else minus_recv).at[k * 4 + d - 1]
-            remote(ref, ref, second_send, recv, partner).wait_recv()
-            if d < 3 or (d == 3 and (k % 2 == 0) == (sign > 0)):
-                push(k, d, sign, ref)
-        remote(ref, ref, cross_send, cross_recv, partner).start()
-
-    events = []
-    for k in range(N):
-        near = min(k, N - k)
-        events.append((near, 0, k, 1))
-        for d in range(1, 5):
-            for sign in (1, -1):
-                if d < 4 or (k % 2 == 0) == (sign > 0):
-                    events.append((near + d, d, k, sign))
-    events.sort()
-
-    normed_at = len(events) * 5 // 8
-    for number, (_, d, k, sign) in enumerate(events):
-        arrived(k, d, sign)
-        if number == normed_at:
+    thin.start()
+
+    for hop in range(5):
+        for piece in wide.step(hop):
+            remote(piece, piece, cross_send, cross_recv, partner).start()
+        if hop == 2:
             for copy in tok_copies:
                 copy.wait_recv()
             square = jnp.zeros((ROWS, 1), F32)
@@ -370,37 +404,36 @@
             for q in range(NX):
                 t = tok[q].astype(F32)
                 columns = slice(q * 512, (q + 1) * 512)
-                normed[:, columns] = (t * factor * norm_gain[:, columns]).astype(BF16)
-
-    everything = weights.at[:, :, 1 - c]
+                normed[:, columns] = (t * factor * norm_gain_v[:, columns]).astype(BF16)
+        if hop == 3:
+            for _ in thin.step(0):
+                pass
+
+    everything = weights.at[1 - c]
     remote(everything, everything, cross_send, cross_recv, partner).wait_recv()
-
-    outw_copies = []
-    for k in (1, 3, 2):
-        x_ = lax.rem(x + k, NX)
-        outw_copies.append(
-            remote(
-                weights.at[pl.ds(2 * x_, 2), :, :, :, pl.ds(1024, 256)],
-                outw.at[x],
-                outw_send.at[k - 1],
-                outw_recv.at[k - 1],
-                at(x_=x_),
-            )
-        )
-    for copy in outw_copies:
-        copy.start()
-    outw_own = pltpu.make_async_copy(
-        weights.at[pl.ds(2 * x, 2), :, :, :, pl.ds(1024, 256)], outw.at[x], outw_load
-    )
-    outw_own.start()
+    for _ in thin.step(1):
+        pass
+
+    def project_mark():
+        pass
 
     def project(n, carry):
         columns = pl.ds(pl.multiple_of(n * 256, 256), 256)
-        w = weights[:, :, :, :, columns].reshape(MODEL, 256)
+        w = jnp.concatenate(
+            [
+                weights[p, j if p else i, i if p else j, :, columns]
+                for i in range(N)
+                for j in range(N)
+                for p in range(2)
+            ],
+            axis=0,
+        )
         proj[:, columns] = jnp.dot(normed[...], w, preferred_element_type=F32).astype(BF16)
         return carry
 
     lax.fori_loop(0, PROJ // 256, project, 0)
+    for _ in thin.step(2):
+        pass
 
     def part(k):
         return proj[:, 128 * k : 128 * (k + 1)].astype(F32)
@@ -426,8 +459,10 @@
         removal_gain[...],
         removal_bias[...],
         decay_bias[...],
-        extra[...],
+        extra_v[...],
     )
+    for _ in thin.step(3):
+        pass
     reads_a[...] = ra
     reads_b[...] = rb
     head0, head1 = packed_heads(trans_a, trans_b)
@@ -443,6 +478,29 @@
     for k in (4, 3, 5, 2, 6, 1, 7):
         remote(line_y.at[y], line_y.at[y], y_send, y_recv.at[y], at(y_=lax.rem(y + k, N))).start()
 
+    for _ in thin.step(4):
+        pass
+    def outw_copies(p):
+        for k in (1, 3, 2, 0):
+            x_ = lax.rem(x + k, NX)
+            if p:
+                src, dst = outs.at[1, :, pl.ds(2 * x_, 2)], outw1.at[x]
+            else:
+                src, dst = outs.at[0, pl.ds(2 * x_, 2)], outw0.at[x]
+            if k:
+                yield remote(src, dst, outw_send.at[k - 1], outw_recv.at[k - 1], at(x_=x_))
+            else:
+                yield pltpu.make_async_copy(src, dst, outw_load)
+
+    for p in range(2):
+
+        @pl.when(c == p)
+        def _():
+            for copy in outw_copies(p):
+                copy.start()
+
+    outw_waits = list(outw_copies(0))
+
     @pl.when(start)
     def _():
         rim[...] = jnp.zeros_like(rim)
@@ -453,9 +511,9 @@
 
     conv_pad[pl.ds(0, 32)] = rim[...].astype(F32)
     conv_pad[pl.ds(32, ROWS)] = conv_in[...].astype(F32)
-    filtered = conv_bias[...] + conv_kernel[0:1] * conv_pad[pl.ds(2, ROWS)]
+    filtered = conv_bias[...] + conv_kernel_v[0:1] * conv_pad[pl.ds(2, ROWS)]
     for k in range(1, CONV_K):
-        filtered = filtered + conv_kernel[k : k + 1] * conv_pad[pl.ds(2 + k, ROWS)]
+        filtered = filtered + conv_kernel_v[k : k + 1] * conv_pad[pl.ds(2 + k, ROWS)]
     near = jnp.mean(filtered, axis=-1, keepdims=True)
     around = jnp.sum((filtered - near) ** 2, axis=-1, keepdims=True)
     lane = lax.broadcasted_iota(jnp.int32, (ROWS, 128), 1)
@@ -491,6 +549,15 @@
         @pl.when(z + k < N)
         def _():
             copy.start()
+
+    for copy in outw_waits[:3]:
+        copy.wait_recv()
+    outw_waits[3].wait()
+    for p, ref in enumerate((outw0, outw1)):
+
+        @pl.when(c == p)
+        def _():
+            remote(ref, ref, outw_cross_send, outw_cross_recv, partner).start()
 
     for copy in stats_copies:
         copy.wait_recv()
@@ -528,10 +595,21 @@
 
     for copy in conv_copies:
         copy.wait_recv()
-    for copy in outw_copies:
-        copy.wait_recv()
-    outw_own.wait()
-    w_of = lambda q, h: outw[q, :, :, :, :, pl.ds(128 * h, 128)].reshape(512, 128)
+    outw_cross = remote(outw0, outw0, outw_cross_send, outw_cross_recv, partner)
+    outw_cross.wait_recv()
+
+    def w_of(q, h):
+        columns = pl.ds(128 * h, 128)
+        return jnp.concatenate(
+            [
+                (outw1[q, j, i, :, columns] if p else outw0[q, i, j, :, columns])
+                for i in range(2)
+                for j in range(N)
+                for p in range(2)
+            ],
+            axis=0,
+        )
+
     total_out = one_nt(feats_conv[0], w_of(0, 1))
     for q in range(1, NX):
         total_out = total_out + one_nt(feats_conv[q], w_of(q, 1))
@@ -568,15 +646,14 @@
         total_out = total_out + one_nt(feats_scan[q], w_of(q, 0))
     out[...] = total_out.astype(BF16)
 
-    for copies in (tok_copies, outw_copies, stats_copies, conv_copies, scan_copies):
+    for copies in (tok_copies, outw_waits[:3], stats_copies, conv_copies, scan_copies):
         for copy in copies:
             copy.wait_send()
     pair_copy.wait_send()
     state_copy.wait_send()
-    seven = weights.at[pl.ds(0, 7), 0, 0]
-    remote(seven, seven, first_send, first_recv.at[0], partner).wait_send()
-    most = weights.at[pl.ds(0, 7), :, 0]
-    remote(most, most, second_send, plus_recv.at[0], partner).wait_send()
+    wide.drain()
+    thin.drain()
+    outw_cross.wait_send()
     remote(everything, everything, cross_send, cross_recv, partner).wait_send()
     lines = line_y.at[pl.ds(0, 7)]
     remote(lines, lines, y_send, y_recv.at[0], partner).wait_send()
@@ -622,14 +699,19 @@
     return pl.pallas_call(
         kernel,
         out_shape=jax.ShapeDtypeStruct((ROWS, 512), BF16),
-        in_specs=[anywhere] + [inside] + [anywhere] * 8 + [inside] * 11,
+        in_specs=[anywhere] * 12 + [inside] * 4 + [anywhere] + [inside] + [anywhere] + [inside] * 2,
         out_specs=inside,
         scratch_shapes=[
-            pltpu.VMEM((N, N, 2, 16, CHUNK), BF16),
+            pltpu.VMEM((2, N, N, 16, PROJ), BF16),
+            pltpu.VMEM((2, N, N, 16, 256), BF16),
+            pltpu.VMEM((ROWS, 128), F32),
+            pltpu.VMEM((1, MODEL), F32),
+            pltpu.VMEM((CONV_K, 128), F32),
             pltpu.VMEM((NX, ROWS, 512), BF16),
             pltpu.VMEM((ROWS, MODEL), BF16),
             pltpu.VMEM((ROWS, PROJ), BF16),
-            pltpu.VMEM((NX, 2, N, 2, 16, 256), BF16),
+            pltpu.VMEM((NX, 2, N, 16, 256), BF16),
+            pltpu.VMEM((NX, N, 2, 16, 256), BF16),
             pltpu.VMEM((64, 128), F32),
             pltpu.VMEM((N, 64, 128), F32),
             pltpu.VMEM((N, 64, 128), F32),
@@ -645,14 +727,21 @@
             pltpu.VMEM((ROWS, 128), F32),
             pltpu.VMEM((ROWS, 128), F32),
             pltpu.VMEM((64, 128), F32),
-            dma((9,)),
-            dma((3,)),
-            dma((3,)),
-            dma(()),
-            dma((7,)),
-            dma(()),
-            dma((32,)),
-            dma((32,)),
+            dma((14,)),
+            dma((3,)),
+            dma((3,)),
+            dma(()),
+            dma((8,)),
+            dma(()),
+            dma((8,)),
+            dma((8,)),
+            dma(()),
+            dma(()),
+            dma(()),
+            dma((8,)),
+            dma(()),
+            dma((8,)),
+            dma((8,)),
             dma(()),
             dma(()),
             dma((3,)),
@@ -689,8 +778,8 @@
         gate_weight,
         conv_value_weight,
         conv_gate_weight,
-        out_scan_weight,
-        out_conv_weight,
+        out_scan_weight.T,
+        out_conv_weight.T,
         row(key_gain),
         row(removal_gain),
         row(removal_bias),

time: 76.1 us -> 79.8 us (1.049)
  the two profiles are of different devices: /device:TPU:129 before, /device:TPU:1 now
where the time goes in v2:
time: 79.8 us; the launch traced here: 78.2 us
  Pallas kernels  76.6 us (96%)
  local copies, waits for them, and re-layouts  1.62 us (2%)
    pallas_call x1, Pallas kernels, shards(): pl.pallas_call(kernel, out_shape=jax.ShapeDtypeStruct((ROWS, 512), BF16),...  76.6 us
    unnamed x1, local copies, waits for them, and re-layouts  1.62 us

profile of v2, /device:TPU:1, one launch (start us, length us, event | category | flops | bytes accessed | tf_op | source)
XLA Modules:
  0.0 78.2 jit_solution(14011417114639913666)
XLA Ops:
  0.0 76.6 %shard_map.199 = bf16[192,512]{1,0:T(8,128)(2,1)} custom-call(bf16[192,512]{1,0:T(8,128)(2,1)} %tokens.1, f32[1,2048]{1,0:T(1,128)} %bitcast.10, bf16[16,128]{1,0:T(8,128)(2,1)} %w0.1, bf16[16,128]{1,0:T(8,128)(2,1)} %w1.1, bf16[16,128]{1,0:T(8,128)(2,1)} %w2.1, bf16[16,128]{1,0:T(8,128)(2,1)} %w3.1, bf16[16,128]{1,0:T(8,128)(2,1)} %w4.1, ...), custom_call_target="tpu_custom_call" | custom-call | tf_op jit(solution)/shard_map/pallas_call | solution.py:699
  76.6 1.6 %copy.23 = bf16[192,512]{1,0:T(8,128)(2,1)} copy(bf16[192,512]{1,0:T(8,128)(2,1)} %shard_map.199) | data formatting | bytes 393216

commit v3 on v2

--- a/solution.py
+++ b/solution.py
@@ -77,9 +77,22 @@
     return ((i >> 6) == (j >> 6)).astype(BF16)
 
 
-def local_scan(
-    recept, keys, values, decay_pre, removal_pre, key_gain, removal_gain, removal_bias, decay_bias, extra
-):
+PAIRS, INVERSE, GATHERED, STEP, READ, CHAIN = three, three, three, three, three, three
+PAIRS_NT = three_nt
+
+
+def spread(a):
+    first = lax.broadcasted_iota(jnp.int32, a.shape, 1) < 64
+    return jnp.concatenate([jnp.where(first, a, 0.0), jnp.where(first, 0.0, a)], axis=0)
+
+
+def masks():
+    i, j = iotas(128, 128)
+    same_head = (i >> 6) == (j >> 6)
+    return i, j, same_head
+
+
+def prepared(keys, values, decay_pre, removal_pre, key_gain, removal_gain, removal_bias, decay_bias, extra):
     ones = head_ones()
     rate = sigmoid(decay_bias + decay_pre) * math.exp(-0.5) + extra
     removal = sigmoid(removal_bias + removal_pre)
@@ -89,21 +102,7 @@
     beta = unit * removal
     i, j = iotas(BLOCK, BLOCK)
     lower = (i >= j).astype(BF16)
-
-    lane = lax.broadcasted_iota(jnp.int32, (BLOCK, 128), 1)
-    first = lane < 64
-
-    def spread(a):
-        return jnp.concatenate([jnp.where(first, a, 0.0), jnp.where(first, 0.0, a)], axis=0)
-
-    i, j = iotas(128, 128)
-    same_head = (i >> 6) == (j >> 6)
-    inclusive = same_head & (i >= j)
-    strict = same_head & (i > j)
-    eye = (i == j).astype(F32)
-    sames = [(i >> s) == (j >> s) for s in (3, 4, 5)] + [same_head]
-
-    parts = []
+    blocks = []
     for b in range(BLOCKS):
         rows = slice(b * BLOCK, (b + 1) * BLOCK)
         rate_b = rate[rows]
@@ -112,60 +111,95 @@
         middle = falling[BLOCK // 2 : BLOCK // 2 + 1]
         ending = falling[BLOCK - 1 :]
         up = jnp.exp(middle - falling)
-        alpha_mid = -unit[rows] * jnp.exp(before - middle)
-        recept_mid = recept[rows] * jnp.exp(falling - middle)
+        to_end = jnp.exp(ending - falling)
         beta_mid = beta[rows] * up
         keys_mid = written[rows] * up
-        to_end = jnp.exp(ending - falling)
-        end_decay = jnp.exp(ending)
-        start_alpha = spread(-unit[rows] * jnp.exp(before))
-        start_recept = spread(recept[rows] * jnp.exp(falling))
-        end_beta = spread(beta[rows] * to_end)
-        end_keys = spread(written[rows] * to_end)
-        values_b = spread(values[rows])
-        left = jnp.concatenate([spread(alpha_mid), spread(recept_mid)], axis=0)
-        right = jnp.concatenate([beta_mid, beta_mid, keys_mid, keys_mid], axis=0)
-        pairs = three_nt(left, right)
-        alpha_beta = jnp.where(strict, pairs[:128, :128], 0.0)
-        alpha_keys = jnp.where(strict, pairs[:128, 128:], 0.0)
-        recept_beta = jnp.where(inclusive, pairs[128:, :128], 0.0)
-        recept_keys = jnp.where(inclusive, pairs[128:, 128:], 0.0)
-        local = three(jnp.concatenate([alpha_keys, recept_keys], axis=0), values_b)
-        base = jnp.where(sames[0], alpha_beta, 0.0)
-        inverse = eye + base
-        power = three(base, base)
-        inverse = inverse + three(inverse, power)
-        power = three(power, power)
-        inverse = inverse + three(inverse, power)
-        for s in range(3):
-            off = jnp.where(sames[s + 1] & ~sames[s], alpha_beta, 0.0)
-            inverse = inverse + three(inverse, three(off, inverse))
-        gathered = three(inverse, jnp.concatenate([start_alpha, local[:128]], axis=1))
-        step = three(end_beta.T, gathered)
-        step_a = step[:, :128] + jnp.where(i == j, end_decay, 0.0)
-        step_b = step[:, 128:] + three(end_keys.T, values_b)
-        reads = three(recept_beta, gathered)
-        read_a = reads[:, :128] + start_recept
-        read_b = reads[:, 128:] + local[128:]
-        parts.append(
-            (step_a, step_b, read_a[:64] + read_a[64:], read_b[:64] + read_b[64:])
+        blocks.append(
+            dict(
+                falling=falling,
+                middle=middle,
+                end_decay=jnp.exp(ending),
+                left=spread(-unit[rows] * jnp.exp(before - middle)),
+                right=jnp.concatenate([beta_mid, beta_mid, keys_mid, keys_mid], axis=0),
+                start_alpha=spread(-unit[rows] * jnp.exp(before)),
+                end_beta=spread(beta[rows] * to_end).T,
+                end_keys=spread(written[rows] * to_end).T,
+                values=spread(values[rows]),
+            )
         )
-    trans_a, trans_b = parts[0][0], parts[0][1]
-    reads_a, reads_b = [parts[0][2]], [parts[0][3]]
-    for b in range(1, BLOCKS):
-        step_a, step_b, read_a, read_b = parts[b]
-        both = jnp.concatenate([trans_a, trans_b], axis=1)
-        seen = three(read_a, both)
-        reads_a.append(seen[:, :128])
-        reads_b.append(seen[:, 128:] + read_b)
-        moved = three(step_a, both)
-        trans_a, trans_b = moved[:, :128], moved[:, 128:] + step_b
-    return (
-        trans_a,
-        trans_b,
-        jnp.concatenate(reads_a, axis=0),
-        jnp.concatenate(reads_b, axis=0),
-    )
+    return blocks
+
+
+def inverted(blocks):
+    i, j, same_head = masks()
+    strict = same_head & (i > j)
+    eye = (i == j).astype(F32)
+    sames = [(i >> s) == (j >> s) for s in (3, 4, 5)] + [same_head]
+    for block in blocks:
+        pairs = PAIRS_NT(block["left"], block["right"])
+        block["links"] = jnp.where(strict, pairs[:, :128], 0.0)
+        alpha_keys = jnp.where(strict, pairs[:, 128:], 0.0)
+        block["local"] = PAIRS(alpha_keys, block["values"])
+        block["power"] = base = jnp.where(sames[0], block["links"], 0.0)
+        block["inverse"] = eye + base
+    for _ in range(2):
+        for block in blocks:
+            block["power"] = INVERSE(block["power"], block["power"])
+        for block in blocks:
+            block["inverse"] = block["inverse"] + INVERSE(block["inverse"], block["power"])
+    for s in range(3):
+        for block in blocks:
+            off = jnp.where(sames[s + 1] & ~sames[s], block["links"], 0.0)
+            block["part"] = INVERSE(off, block["inverse"])
+        for block in blocks:
+            block["inverse"] = block["inverse"] + INVERSE(block["inverse"], block["part"])
+
+
+def transition(blocks):
+    i, j, same_head = masks()
+    for block in blocks:
+        block["gathered"] = GATHERED(
+            block["inverse"], jnp.concatenate([block["start_alpha"], block["local"]], axis=1)
+        )
+    for block in blocks:
+        step = STEP(block["end_beta"], block["gathered"])
+        block["step_a"] = step[:, :128] + jnp.where(i == j, block["end_decay"], 0.0)
+        block["step_b"] = step[:, 128:] + STEP(block["end_keys"], block["values"])
+    both = jnp.concatenate([blocks[0]["step_a"], blocks[0]["step_b"]], axis=1)
+    for block in blocks[1:]:
+        block["start"] = both
+        moved = CHAIN(block["step_a"], both)
+        both = jnp.concatenate([moved[:, :128], moved[:, 128:] + block["step_b"]], axis=1)
+    return both[:, :128], both[:, 128:]
+
+
+def read_parts(blocks, recept):
+    i, j, same_head = masks()
+    inclusive = same_head & (i >= j)
+    reads_a, reads_b = [], []
+    for b, block in enumerate(blocks):
+        rows = slice(b * BLOCK, (b + 1) * BLOCK)
+        left = spread(recept[rows] * jnp.exp(block["falling"] - block["middle"]))
+        pairs = PAIRS_NT(left, block["right"])
+        recept_beta = jnp.where(inclusive, pairs[:, :128], 0.0)
+        recept_keys = jnp.where(inclusive, pairs[:, 128:], 0.0)
+        reads = READ(recept_beta, block["gathered"])
+        read_a = reads[:64, :128] + reads[64:, :128] + recept[rows] * jnp.exp(block["falling"])
+        read_b = reads[:, 128:] + READ(recept_keys, block["values"])
+        read_b = read_b[:64] + read_b[64:]
+        if b:
+            seen = READ(read_a, block["start"])
+            read_a, read_b = seen[:, :128], seen[:, 128:] + read_b
+        reads_a.append(read_a)
+        reads_b.append(read_b)
+    return jnp.concatenate(reads_a, axis=0), jnp.concatenate(reads_b, axis=0)
+
+
+def local_scan(recept, keys, values, decay_pre, removal_pre, *rest):
+    blocks = prepared(keys, values, decay_pre, removal_pre, *rest)
+    inverted(blocks)
+    trans = transition(blocks)
+    return (*trans, *read_parts(blocks, recept))
 
 
 def packed_heads(trans_a, trans_b):
@@ -175,9 +209,35 @@
     return head0, head1
 
 
+def coded(both):
+    i, j = iotas(64, 128)
+    on = i == j
+    diagonal = jnp.sum(jnp.where(on, both, 0.0), axis=0, keepdims=True)
+    high, rest = split2(diagonal)
+    low = (diagonal - high.astype(F32) - rest.astype(F32)).astype(BF16)
+    row = lax.broadcasted_iota(jnp.int32, (16, 128), 0)
+    below = jnp.where(
+        row == 0,
+        high.astype(F32),
+        jnp.where(row == 1, rest.astype(F32), jnp.where(row == 2, low.astype(F32), 0.0)),
+    )
+    return jnp.concatenate([jnp.where(on, 0.0, both), below], axis=0).astype(BF16)
+
+
+def decoded(code):
+    code = code.astype(F32)
+    i, j = iotas(64, 128)
+    diagonal = code[64:65] + code[65:66] + code[66:67]
+    return jnp.where(i == j, diagonal, code[:64])
+
+
 def combine(later, total):
     lane = lax.broadcasted_iota(jnp.int32, later.shape, 1)
     return three(later[:, :64], total) + jnp.where(lane < 64, 0.0, later)
+
+
+NORM_AT = 11
+THIN_AT = 3
 
 
 def kernel(
@@ -245,6 +305,8 @@
     minus_recv2,
     outw_cross_send,
     outw_cross_recv,
+    late_send,
+    late_recv,
     outw_send,
     outw_recv,
     outw_load,
@@ -284,13 +346,13 @@
     loads = [
         pltpu.make_async_copy(tokens, tok.at[x], load_sem.at[0]),
     ]
-    for k, w in enumerate((w0, w1, w2, w3, w4, w5, w6, w7)):
+    for k, w in enumerate((w1, w2, w3, w4)):
         loads.append(
             pltpu.make_async_copy(w, weights.at[c, b, a, :, pl.ds(128 * k, 128)], load_sem.at[k + 1])
         )
-    for k, w in enumerate((out_scan, out_conv)):
+    for k, w in enumerate((w0, w5, w6, w7, out_scan, out_conv)):
         loads.append(
-            pltpu.make_async_copy(w, outs.at[c, b, a, :, pl.ds(128 * k, 128)], load_sem.at[k + 9])
+            pltpu.make_async_copy(w, outs.at[c, b, a, :, pl.ds(128 * k, 128)], load_sem.at[k + 5])
         )
     loads.append(pltpu.make_async_copy(extra, extra_v, load_sem.at[11]))
     loads.append(pltpu.make_async_copy(norm_gain, norm_gain_v, load_sem.at[12]))
@@ -332,50 +394,64 @@
         def __init__(self, ref, first_send, first_recv, second_send, plus_recv, minus_recv):
             self.ref, self.first_send, self.first_recv = ref, first_send, first_recv
             self.second_send, self.recvs = second_send, {1: plus_recv, -1: minus_recv}
-            self.own_half = (a // 4) * 4
 
         def start(self):
             own = self.ref.at[c, b, a]
             for k in (1, 7, 2, 6, 3, 5, 4):
                 remote(own, own, self.first_send, self.first_recv.at[a], along_first(k)).start()
 
-        def half(self, h, distance):
-            low = self.own_half if h == 0 else 4 - self.own_half
-            return self.ref.at[c, lax.rem(b + distance + N, N), pl.ds(low, 4)]
-
-        def copy(self, h, distance, sign, hop):
-            piece = self.half(h, distance)
-            recv = self.recvs[sign].at[h * 4 + hop]
-            return remote(piece, piece, self.second_send, recv, along_second(1 if sign > 0 else N - 1))
+        def low(self, h):
+            return lax.rem(a // 2 + h, 4) * 2
+
+        def piece(self, h, distance):
+            return self.ref.at[c, lax.rem(b + distance + N, N), pl.ds(self.low(h), 2)]
+
+        def copy(self, h, source, sign, reach):
+            piece = self.piece(h, -sign * source)
+            recv = self.recvs[sign].at[h * 4 + source + reach - 1]
+            target = along_second(reach if sign > 0 else N - reach)
+            return remote(piece, piece, self.second_send, recv, target)
 
         def collect(self, h):
-            low = self.own_half if h == 0 else 4 - self.own_half
-            for k in range(4):
-                a_ = low + k
-
-                @pl.when(a_ != a)
-                def _():
+            for k in range(2):
+                a_ = self.low(h) + k
+
+                def wait():
                     piece = self.ref.at[c, b, a_]
                     remote(piece, piece, self.first_send, self.first_recv.at[a_], partner).wait_recv()
 
+                if h:
+                    wait()
+                else:
+                    pl.when(a_ != a)(wait)
+
+            for reach in (2, 1):
+                for sign in (1, -1):
+                    self.copy(h, 0, sign, reach).start()
+            return [self.piece(h, 0)]
+
+        def has_far(self, h, sign):
+            return (h % 2 == 0) == (sign > 0)
+
+        def arrive(self, h, d, sign):
+            self.copy(h, 0, sign, d).wait_recv()
+            return self.piece(h, -sign * d)
+
+        def relay(self, h):
+            pieces = []
             for sign in (1, -1):
-                self.copy(h, 0, sign, 0).start()
-            return self.half(h, 0)
-
-        def moved(self, h, hop, sign):
-            self.copy(h, -sign * hop, sign, hop - 1).wait_recv()
-            if hop < 3 or (hop == 3 and (h == 0) == (sign > 0)):
-                self.copy(h, -sign * hop, sign, hop).start()
-            return self.half(h, -sign * hop)
-
-        def step(self, hop):
-            for h in (0, 1):
-                if hop == 0:
-                    yield self.collect(h)
-                    continue
-                for sign in (1, -1):
-                    if hop < 4 or (h == 0) == (sign > 0):
-                        yield self.moved(h, hop, sign)
+                pieces.append(self.arrive(h, 2, sign))
+                if self.has_far(h, sign):
+                    self.copy(h, 2, sign, 2).start()
+                self.copy(h, 2, sign, 1).start()
+            return pieces
+
+        def near(self, h):
+            return [self.arrive(h, 1, sign) for sign in (1, -1)]
+
+        def far(self, h):
+            pieces = [self.arrive(h, 4, sign) for sign in (1, -1) if self.has_far(h, sign)]
+            return pieces + [self.arrive(h, 3, sign) for sign in (1, -1)]
 
         def drain(self):
             seven = self.ref.at[0, 0, pl.ds(0, 7)]
@@ -388,12 +464,18 @@
     wide.start()
     for copy in tok_copies:
         copy.start()
-    thin.start()
-
-    for hop in range(5):
-        for piece in wide.step(hop):
+
+    order = (0, 1, 3, 2)
+    events = [(wide.collect, h) for h in order]
+    for h in order:
+        events += [(wide.relay, h), (wide.near, h)]
+    events += [(wide.far, h) for h in order]
+    for number, (event, h) in enumerate(events):
+        for piece in event(h):
             remote(piece, piece, cross_send, cross_recv, partner).start()
-        if hop == 2:
+        if number == THIN_AT:
+            thin.start()
+        if number == NORM_AT:
             for copy in tok_copies:
                 copy.wait_recv()
             square = jnp.zeros((ROWS, 1), F32)
@@ -405,66 +487,51 @@
                 t = tok[q].astype(F32)
                 columns = slice(q * 512, (q + 1) * 512)
                 normed[:, columns] = (t * factor * norm_gain_v[:, columns]).astype(BF16)
-        if hop == 3:
-            for _ in thin.step(0):
-                pass
 
     everything = weights.at[1 - c]
     remote(everything, everything, cross_send, cross_recv, partner).wait_recv()
-    for _ in thin.step(1):
-        pass
-
-    def project_mark():
-        pass
-
-    def project(n, carry):
-        columns = pl.ds(pl.multiple_of(n * 256, 256), 256)
-        w = jnp.concatenate(
-            [
-                weights[p, j if p else i, i if p else j, :, columns]
-                for i in range(N)
-                for j in range(N)
-                for p in range(2)
-            ],
-            axis=0,
-        )
-        proj[:, columns] = jnp.dot(normed[...], w, preferred_element_type=F32).astype(BF16)
-        return carry
-
-    lax.fori_loop(0, PROJ // 256, project, 0)
-    for _ in thin.step(2):
-        pass
+    for h in order:
+        thin.collect(h)
+
+    def project(ref, base):
+        def columns_of(n, carry):
+            columns = pl.ds(pl.multiple_of(n * 256, 256), 256)
+            w = jnp.concatenate(
+                [
+                    ref[p, j if p else i, i if p else j, :, columns]
+                    for i in range(N)
+                    for j in range(N)
+                    for p in range(2)
+                ],
+                axis=0,
+            )
+            proj[:, pl.ds(pl.multiple_of(base + n * 256, 256), 256)] = jnp.dot(
+                normed[...], w, preferred_element_type=F32
+            ).astype(BF16)
+            return carry
+
+        lax.fori_loop(0, 2, columns_of, 0)
+
+    project(weights, 0)
 
     def part(k):
         return proj[:, 128 * k : 128 * (k + 1)].astype(F32)
 
-    conv_in[...] = (part(6) * sigmoid(part(7))).astype(BF16)
-    last = place == size - 1
-    start = place == 0
-    rim_copy = remote(
-        conv_in.at[pl.ds(ROWS - 32, 32)], rim, rim_send, rim_recv, as_device(after)
-    )
-
-    @pl.when(jnp.logical_not(last))
-    def _():
-        rim_copy.start()
-
-    trans_a, trans_b, ra, rb = local_scan(
+    blocks = prepared(
         part(0),
         part(1),
         part(2),
         part(3),
-        part(4),
         key_gain[...],
         removal_gain[...],
         removal_bias[...],
         decay_bias[...],
         extra_v[...],
     )
-    for _ in thin.step(3):
-        pass
-    reads_a[...] = ra
-    reads_b[...] = rb
+    inverted(blocks)
+    trans_a, trans_b = transition(blocks)
+    for h in order:
+        thin.relay(h)
     head0, head1 = packed_heads(trans_a, trans_b)
     upper = c == 1
     pair_out[...] = jnp.where(upper, head0, head1)
@@ -474,19 +541,24 @@
     pair_copy.wait_recv()
     earlier = jnp.where(upper, pair_in[...], mine[...])
     later = jnp.where(upper, mine[...], pair_in[...])
-    line_y[y] = combine(later, earlier)
+    line_y[y] = coded(combine(later, earlier))
     for k in (4, 3, 5, 2, 6, 1, 7):
         remote(line_y.at[y], line_y.at[y], y_send, y_recv.at[y], at(y_=lax.rem(y + k, N))).start()
 
-    for _ in thin.step(4):
-        pass
+    for h in order:
+        thin.near(h)
+        thin.far(h)
+    own_paths = outs.at[c, :, :, :, pl.ds(0, 512)]
+    other_paths = outs.at[1 - c, :, :, :, pl.ds(0, 512)]
+    late_cross = remote(own_paths, own_paths, late_send, late_recv, partner)
+    late_cross.start()
     def outw_copies(p):
         for k in (1, 3, 2, 0):
             x_ = lax.rem(x + k, NX)
             if p:
-                src, dst = outs.at[1, :, pl.ds(2 * x_, 2)], outw1.at[x]
+                src, dst = outs.at[1, :, pl.ds(2 * x_, 2), :, pl.ds(512, 256)], outw1.at[x]
             else:
-                src, dst = outs.at[0, pl.ds(2 * x_, 2)], outw0.at[x]
+                src, dst = outs.at[0, pl.ds(2 * x_, 2), :, :, pl.ds(512, 256)], outw0.at[x]
             if k:
                 yield remote(src, dst, outw_send.at[k - 1], outw_recv.at[k - 1], at(x_=x_))
             else:
@@ -500,6 +572,20 @@
                 copy.start()
 
     outw_waits = list(outw_copies(0))
+
+    remote(other_paths, other_paths, late_send, late_recv, partner).wait_recv()
+    project(outs, 512)
+
+    conv_in[...] = (part(6) * sigmoid(part(7))).astype(BF16)
+    last = place == size - 1
+    start = place == 0
+    rim_copy = remote(conv_in.at[pl.ds(ROWS - 32, 32)], rim, rim_send, rim_recv, as_device(after))
+
+    @pl.when(jnp.logical_not(last))
+    def _():
+        rim_copy.start()
+
+    reads_a[...], reads_b[...] = read_parts(blocks, part(4))
 
     @pl.when(start)
     def _():
@@ -536,9 +622,9 @@
         def _():
             remote(line_y.at[k], line_y.at[k], y_send, y_recv.at[k], partner).wait_recv()
 
-        total = combine(line_y[k], total)
+        total = combine(decoded(line_y[k]), total)
         inside = jnp.where(k < y, total, inside)
-    line_z[z] = total
+    line_z[z] = coded(total)
     z_copies = []
     for k in range(N - 1, 0, -1):
         copy = remote(
@@ -583,7 +669,7 @@
 
     def advance(k, state):
         remote(line_z.at[k], line_z.at[k], z_send.at[0], z_recv.at[k], partner).wait_recv()
-        return combine(line_z[k], state)
+        return combine(decoded(line_z[k]), state)
 
     state = lax.fori_loop(0, z, advance, jnp.zeros((64, 128), F32))
     state = jnp.where(lane < 64, 0.0, combine(inside, state))
@@ -654,6 +740,7 @@
     wide.drain()
     thin.drain()
     outw_cross.wait_send()
+    late_cross.wait_send()
     remote(everything, everything, cross_send, cross_recv, partner).wait_send()
     lines = line_y.at[pl.ds(0, 7)]
     remote(lines, lines, y_send, y_recv.at[0], partner).wait_send()
@@ -702,8 +789,8 @@
         in_specs=[anywhere] * 12 + [inside] * 4 + [anywhere] + [inside] + [anywhere] + [inside] * 2,
         out_specs=inside,
         scratch_shapes=[
-            pltpu.VMEM((2, N, N, 16, PROJ), BF16),
-            pltpu.VMEM((2, N, N, 16, 256), BF16),
+            pltpu.VMEM((2, N, N, 16, 512), BF16),
+            pltpu.VMEM((2, N, N, 16, 768), BF16),
             pltpu.VMEM((ROWS, 128), F32),
             pltpu.VMEM((1, MODEL), F32),
             pltpu.VMEM((CONV_K, 128), F32),
@@ -713,8 +800,8 @@
             pltpu.VMEM((NX, 2, N, 16, 256), BF16),
             pltpu.VMEM((NX, N, 2, 16, 256), BF16),
             pltpu.VMEM((64, 128), F32),
-            pltpu.VMEM((N, 64, 128), F32),
-            pltpu.VMEM((N, 64, 128), F32),
+            pltpu.VMEM((N, 80, 128), BF16),
+            pltpu.VMEM((N, 80, 128), BF16),
             pltpu.VMEM((64, 128), F32),
             pltpu.VMEM((64, 128), F32),
             pltpu.VMEM((64, 128), F32),
@@ -733,15 +820,17 @@
             dma(()),
             dma((8,)),
             dma(()),
+            dma((16,)),
+            dma((16,)),
+            dma(()),
+            dma(()),
+            dma(()),
             dma((8,)),
-            dma((8,)),
-            dma(()),
-            dma(()),
-            dma(()),
-            dma((8,)),
-            dma(()),
-            dma((8,)),
-            dma((8,)),
+            dma(()),
+            dma((16,)),
+            dma((16,)),
+            dma(()),
+            dma(()),
             dma(()),
             dma(()),
             dma((3,)),

time: 79.8 us -> 71.2 us (0.89); the launches traced: 78.2 us -> 70.9 us
  Pallas kernels: 76.6 us -> 69.3 us
    pallas_call x1, Pallas kernels: 76.6 us -> 69.3 us  [shards(): pl.pallas_call(kernel, out_shape=jax.ShapeDtypeStruct((ROWS, 512), BF16),...]
where the time goes in v3:
time: 71.2 us; the launch traced here: 70.9 us
  Pallas kernels  69.3 us (97%)
  local copies, waits for them, and re-layouts  1.62 us (2%)
    pallas_call x1, Pallas kernels, shards(): pl.pallas_call(kernel, out_shape=jax.ShapeDtypeStruct((ROWS, 512), BF16),...  69.3 us
    unnamed x1, local copies, waits for them, and re-layouts  1.62 us

profile of v3, /device:TPU:1, one launch (start us, length us, event | category | flops | bytes accessed | tf_op | source)
XLA Modules:
  0.0 70.9 jit_solution(3689529115613590307)
XLA Ops:
  0.0 69.3 %shard_map.199 = bf16[192,512]{1,0:T(8,128)(2,1)} custom-call(bf16[192,512]{1,0:T(8,128)(2,1)} %tokens.1, f32[1,2048]{1,0:T(1,128)} %bitcast.10, bf16[16,128]{1,0:T(8,128)(2,1)} %w0.1, bf16[16,128]{1,0:T(8,128)(2,1)} %w1.1, bf16[16,128]{1,0:T(8,128)(2,1)} %w2.1, bf16[16,128]{1,0:T(8,128)(2,1)} %w3.1, bf16[16,128]{1,0:T(8,128)(2,1)} %w4.1, ...), custom_call_target="tpu_custom_call" | custom-call | tf_op jit(solution)/shard_map/pallas_call | solution.py:786
  69.3 1.6 %copy.23 = bf16[192,512]{1,0:T(8,128)(2,1)} copy(bf16[192,512]{1,0:T(8,128)(2,1)} %shard_map.199) | data formatting | bytes 393216

commit v4 on v3

--- a/solution.py
+++ b/solution.py
@@ -77,8 +77,8 @@
     return ((i >> 6) == (j >> 6)).astype(BF16)
 
 
-PAIRS, INVERSE, GATHERED, STEP, READ, CHAIN = three, three, three, three, three, three
-PAIRS_NT = three_nt
+PAIRS, INVERSE, GATHERED, STEP, READ, CHAIN = one, one, one, one, one, three
+PAIRS_NT = one_nt
 
 
 def spread(a):
@@ -469,10 +469,12 @@
     events = [(wide.collect, h) for h in order]
     for h in order:
         events += [(wide.relay, h), (wide.near, h)]
+    events += [(thin.collect, h) for h in order]
     events += [(wide.far, h) for h in order]
     for number, (event, h) in enumerate(events):
         for piece in event(h):
-            remote(piece, piece, cross_send, cross_recv, partner).start()
+            if event.__self__ is wide:
+                remote(piece, piece, cross_send, cross_recv, partner).start()
         if number == THIN_AT:
             thin.start()
         if number == NORM_AT:
@@ -490,8 +492,6 @@
 
     everything = weights.at[1 - c]
     remote(everything, everything, cross_send, cross_recv, partner).wait_recv()
-    for h in order:
-        thin.collect(h)
 
     def project(ref, base):
         def columns_of(n, carry):
@@ -530,8 +530,6 @@
     )
     inverted(blocks)
     trans_a, trans_b = transition(blocks)
-    for h in order:
-        thin.relay(h)
     head0, head1 = packed_heads(trans_a, trans_b)
     upper = c == 1
     pair_out[...] = jnp.where(upper, head0, head1)
@@ -544,6 +542,33 @@
     line_y[y] = coded(combine(later, earlier))
     for k in (4, 3, 5, 2, 6, 1, 7):
         remote(line_y.at[y], line_y.at[y], y_send, y_recv.at[y], at(y_=lax.rem(y + k, N))).start()
+
+    for h in order:
+        thin.relay(h)
+
+    lane = lax.broadcasted_iota(jnp.int32, (64, 128), 1)
+    i, j = iotas(64, 128)
+    blank = (i == j).astype(F32)
+    total = inside = blank
+    for k in range(N):
+
+        @pl.when(y != k)
+        def _():
+            remote(line_y.at[k], line_y.at[k], y_send, y_recv.at[k], partner).wait_recv()
+
+        total = combine(decoded(line_y[k]), total)
+        inside = jnp.where(k < y, total, inside)
+    line_z[z] = coded(total)
+    z_copies = []
+    for k in range(N - 1, 0, -1):
+        copy = remote(
+            line_z.at[z], line_z.at[z], z_send.at[k - 1], z_recv.at[z], at(z_=lax.rem(z + k, N))
+        )
+        z_copies.append((k, copy))
+
+        @pl.when(z + k < N)
+        def _():
+            copy.start()
 
     for h in order:
         thin.near(h)
@@ -603,7 +628,7 @@
     near = jnp.mean(filtered, axis=-1, keepdims=True)
     around = jnp.sum((filtered - near) ** 2, axis=-1, keepdims=True)
     lane = lax.broadcasted_iota(jnp.int32, (ROWS, 128), 1)
-    stats[x] = jnp.where(lane < 64, near, around)
+    stats[x] = jnp.where(lane == 0, near, jnp.where(lane == 1, around, 0.0)).T[:8]
     conv_pad[pl.ds(0, ROWS)] = filtered
     stats_copies = [
         remote(stats.at[x], stats.at[x], stats_send.at[k - 1], stats_recv.at[k - 1], at(x_=lax.rem(x + k, NX)))
@@ -612,30 +637,6 @@
     for copy in stats_copies:
         copy.start()
 
-    lane = lax.broadcasted_iota(jnp.int32, (64, 128), 1)
-    i, j = iotas(64, 128)
-    blank = (i == j).astype(F32)
-    total = inside = blank
-    for k in range(N):
-
-        @pl.when(y != k)
-        def _():
-            remote(line_y.at[k], line_y.at[k], y_send, y_recv.at[k], partner).wait_recv()
-
-        total = combine(decoded(line_y[k]), total)
-        inside = jnp.where(k < y, total, inside)
-    line_z[z] = coded(total)
-    z_copies = []
-    for k in range(N - 1, 0, -1):
-        copy = remote(
-            line_z.at[z], line_z.at[z], z_send.at[k - 1], z_recv.at[z], at(z_=lax.rem(z + k, N))
-        )
-        z_copies.append((k, copy))
-
-        @pl.when(z + k < N)
-        def _():
-            copy.start()
-
     for copy in outw_waits[:3]:
         copy.wait_recv()
     outw_waits[3].wait()
@@ -645,18 +646,19 @@
         def _():
             remote(ref, ref, outw_cross_send, outw_cross_recv, partner).start()
 
+    lane = lax.broadcasted_iota(jnp.int32, (64, 128), 1)
+
     for copy in stats_copies:
         copy.wait_recv()
-    center = jnp.zeros((ROWS, 1), F32)
+    center = sum(stats[q][0:1] for q in range(NX)) * (1.0 / NX)
+    spread_row = jnp.zeros((1, ROWS), F32)
     for q in range(NX):
-        center = center + stats[q][:, 0:1]
-    center = center * (1.0 / NX)
-    spread = jnp.zeros((ROWS, 1), F32)
-    for q in range(NX):
-        gap = stats[q][:, 0:1] - center
-        spread = spread + stats[q][:, 64:65] + 128.0 * gap * gap
-    spread = spread * (1.0 / 512.0)
-    normal = (conv_pad[pl.ds(0, ROWS)] - center) * lax.rsqrt(spread + 1e-05) * conv_norm_gain[...]
+        gap = stats[q][0:1] - center
+        spread_row = spread_row + stats[q][1:2] + 128.0 * gap * gap
+    row = lax.broadcasted_iota(jnp.int32, (8, ROWS), 0)
+    scale_row = lax.rsqrt(spread_row * (1.0 / 512.0) + 1e-05)
+    column = jnp.where(row == 0, center, jnp.where(row == 1, scale_row, 0.0)).T
+    normal = (conv_pad[pl.ds(0, ROWS)] - column[:, 0:1]) * column[:, 1:2] * conv_norm_gain[...]
     feats_conv[x] = (normal * sigmoid(normal)).astype(BF16)
     conv_copies = [
         remote(
@@ -808,7 +810,7 @@
             pltpu.VMEM((32, 128), BF16),
             pltpu.VMEM((ROWS, 128), BF16),
             pltpu.VMEM((ROWS + 32, 128), F32),
-            pltpu.VMEM((NX, ROWS, 128), F32),
+            pltpu.VMEM((NX, 8, ROWS), F32),
             pltpu.VMEM((NX, ROWS, 128), BF16),
             pltpu.VMEM((NX, ROWS, 128), BF16),
             pltpu.VMEM((ROWS, 128), F32),

time: 71.2 us -> 67.4 us (0.947)
  Pallas kernels: 69.3 us -> 65 us
    pallas_call x1, Pallas kernels: 69.3 us -> 65 us  [shards(): pl.pallas_call(kernel, out_shape=jax.ShapeDtypeStruct((ROWS, 512), BF16),...]
where the time goes in v4:
time: 67.4 us; the launch traced here: 66.7 us
  Pallas kernels  65 us (96%)
  local copies, waits for them, and re-layouts  1.62 us (2%)
    pallas_call x1, Pallas kernels, shards(): pl.pallas_call(kernel, out_shape=jax.ShapeDtypeStruct((ROWS, 512), BF16),...  65 us
    unnamed x1, local copies, waits for them, and re-layouts  1.62 us

profile of v4, /device:TPU:1, one launch (start us, length us, event | category | flops | bytes accessed | tf_op | source)
XLA Modules:
  0.0 66.7 jit_solution(230793735536693839)
XLA Ops:
  0.0 65.0 %shard_map.199 = bf16[192,512]{1,0:T(8,128)(2,1)} custom-call(bf16[192,512]{1,0:T(8,128)(2,1)} %tokens.1, f32[1,2048]{1,0:T(1,128)} %bitcast.10, bf16[16,128]{1,0:T(8,128)(2,1)} %w0.1, bf16[16,128]{1,0:T(8,128)(2,1)} %w1.1, bf16[16,128]{1,0:T(8,128)(2,1)} %w2.1, bf16[16,128]{1,0:T(8,128)(2,1)} %w3.1, bf16[16,128]{1,0:T(8,128)(2,1)} %w4.1, ...), custom_call_target="tpu_custom_call" | custom-call | tf_op jit(solution)/shard_map/pallas_call | solution.py:788
  65.0 1.6 %copy.23 = bf16[192,512]{1,0:T(8,128)(2,1)} copy(bf16[192,512]{1,0:T(8,128)(2,1)} %shard_map.199) | data formatting | bytes 393216

commit v5 on v4

v5 whole, which is shorter than its diff:
```python
import functools
import math

import jax
import jax.numpy as jnp
from jax import lax
from jax.experimental import pallas as pl
from jax.experimental.pallas import tpu as pltpu
from jax.sharding import Mesh
from jax.sharding import PartitionSpec as P

F32 = jnp.float32
BF16 = jnp.bfloat16
SP = ("sp_0", "sp_1", "sp_2")
MESH = pl.DeviceIdType.MESH
CONV_K = 31
ROWS = 192
BLOCK = 64
BLOCKS = ROWS // BLOCK
MODEL = 2048
NX = 4
PROJ = 1024
N = 8


def split2(a):
    high = a.astype(BF16)
    return high, (a - high.astype(F32)).astype(BF16)


def one(a, b):
    return jnp.dot(a.astype(BF16), b.astype(BF16), preferred_element_type=F32)


def one_nt(a, b):
    return lax.dot_general(
        a.astype(BF16), b.astype(BF16), (((1,), (1,)), ((), ())), preferred_element_type=F32
    )


def three(a, b):
    ah, al = split2(a)
    bh, bl = split2(b)
    return one(ah, bh) + one(al, bh) + one(ah, bl)


def three_nt(a, b):
    ah, al = split2(a)
    bh, bl = split2(b)
    return one_nt(ah, bh) + one_nt(al, bh) + one_nt(ah, bl)


def left_exact(a, b):
    bh, bm = split2(b)
    bl = (b - bh.astype(F32) - bm.astype(F32)).astype(BF16)
    return one(a, bh) + one(a, bm) + one(a, bl)


def right_exact(a, b):
    ah, al = split2(a)
    return one(ah, b) + one(al, b)


def iotas(rows, columns):
    return (
        lax.broadcasted_iota(jnp.int32, (rows, columns), 0),
        lax.broadcasted_iota(jnp.int32, (rows, columns), 1),
    )


def sigmoid(x):
    return 1.0 / (1.0 + jnp.exp(-x))


def head_ones():
    i, j = iotas(128, 128)
    return ((i >> 6) == (j >> 6)).astype(BF16)


PAIRS, INVERSE, GATHERED, STEP, READ, CHAIN = one, one, one, one, one, three
PAIRS_NT = one_nt


def spread(a):
    first = lax.broadcasted_iota(jnp.int32, a.shape, 1) < 64
    return jnp.concatenate([jnp.where(first, a, 0.0), jnp.where(first, 0.0, a)], axis=0)


def masks():
    i, j = iotas(128, 128)
    same_head = (i >> 6) == (j >> 6)
    return i, j, same_head


def prepared(keys, values, decay_pre, removal_pre, key_gain, removal_gain, removal_bias, decay_bias, extra):
    ones = head_ones()
    rate = sigmoid(decay_bias + decay_pre) * math.exp(-0.5) + extra
    removal = sigmoid(removal_bias + removal_pre)
    scaled = keys * key_gain
    unit = scaled * lax.rsqrt(right_exact(scaled * scaled, ones) + 1e-06)
    written = keys * (1.0 + (removal - 1.0) * removal_gain)
    beta = unit * removal
    i, j = iotas(BLOCK, BLOCK)
    lower = (i >= j).astype(BF16)
    blocks = []
    for b in range(BLOCKS):
        rows = slice(b * BLOCK, (b + 1) * BLOCK)
        rate_b = rate[rows]
        falling = -left_exact(lower, rate_b)
        before = falling + rate_b
        middle = falling[BLOCK // 2 : BLOCK // 2 + 1]
        ending = falling[BLOCK - 1 :]
        up = jnp.exp(middle - falling)
        to_end = jnp.exp(ending - falling)
        beta_mid = beta[rows] * up
        keys_mid = written[rows] * up
        blocks.append(
            dict(
                falling=falling,
                middle=middle,
                end_decay=jnp.exp(ending),
                left=spread(-unit[rows] * jnp.exp(before - middle)),
                right=jnp.concatenate([beta_mid, beta_mid, keys_mid, keys_mid], axis=0),
                start_alpha=spread(-unit[rows] * jnp.exp(before)),
                end_beta=spread(beta[rows] * to_end).T,
                end_keys=spread(written[rows] * to_end).T,
                values=spread(values[rows]),
            )
        )
    return blocks


def inverted(blocks):
    i, j, same_head = masks()
    strict = same_head & (i > j)
    eye = (i == j).astype(F32)
    sames = [(i >> s) == (j >> s) for s in (3, 4, 5)] + [same_head]
    for block in blocks:
        pairs = PAIRS_NT(block["left"], block["right"])
        block["links"] = jnp.where(strict, pairs[:, :128], 0.0)
        alpha_keys = jnp.where(strict, pairs[:, 128:], 0.0)
        block["local"] = PAIRS(alpha_keys, block["values"])
        block["power"] = base = jnp.where(sames[0], block["links"], 0.0)
        block["inverse"] = eye + base
    for _ in range(2):
        for block in blocks:
            block["power"] = INVERSE(block["power"], block["power"])
        for block in blocks:
            block["inverse"] = block["inverse"] + INVERSE(block["inverse"], block["power"])
    for s in range(3):
        for block in blocks:
            off = jnp.where(sames[s + 1] & ~sames[s], block["links"], 0.0)
            block["part"] = INVERSE(off, block["inverse"])
        for block in blocks:
            block["inverse"] = block["inverse"] + INVERSE(block["inverse"], block["part"])


def transition(blocks):
    i, j, same_head = masks()
    for block in blocks:
        block["gathered"] = GATHERED(
            block["inverse"], jnp.concatenate([block["start_alpha"], block["local"]], axis=1)
        )
    for block in blocks:
        step = STEP(block["end_beta"], block["gathered"])
        block["step_a"] = step[:, :128] + jnp.where(i == j, block["end_decay"], 0.0)
        block["step_b"] = step[:, 128:] + STEP(block["end_keys"], block["values"])
    both = jnp.concatenate([blocks[0]["step_a"], blocks[0]["step_b"]], axis=1)
    for block in blocks[1:]:
        block["start"] = both
        moved = CHAIN(block["step_a"], both)
        both = jnp.concatenate([moved[:, :128], moved[:, 128:] + block["step_b"]], axis=1)
    return both[:, :128], both[:, 128:]


def read_parts(blocks, recept):
    i, j, same_head = masks()
    inclusive = same_head & (i >= j)
    reads_a, reads_b = [], []
    for b, block in enumerate(blocks):
        rows = slice(b * BLOCK, (b + 1) * BLOCK)
        left = spread(recept[rows] * jnp.exp(block["falling"] - block["middle"]))
        pairs = PAIRS_NT(left, block["right"])
        recept_beta = jnp.where(inclusive, pairs[:, :128], 0.0)
        recept_keys = jnp.where(inclusive, pairs[:, 128:], 0.0)
        reads = READ(recept_beta, block["gathered"])
        read_a = reads[:64, :128] + reads[64:, :128] + recept[rows] * jnp.exp(block["falling"])
        read_b = reads[:, 128:] + READ(recept_keys, block["values"])
        read_b = read_b[:64] + read_b[64:]
        if b:
            seen = READ(read_a, block["start"])
            read_a, read_b = seen[:, :128], seen[:, 128:] + read_b
        reads_a.append(read_a)
        reads_b.append(read_b)
    return jnp.concatenate(reads_a, axis=0), jnp.concatenate(reads_b, axis=0)


def local_scan(recept, keys, values, decay_pre, removal_pre, *rest):
    blocks = prepared(keys, values, decay_pre, removal_pre, *rest)
    inverted(blocks)
    trans = transition(blocks)
    return (*trans, *read_parts(blocks, recept))


def packed_heads(trans_a, trans_b):
    lane = lax.broadcasted_iota(jnp.int32, (64, 128), 1)
    head0 = jnp.where(lane < 64, trans_a[:64], pltpu.roll(trans_b[:64], 64, 1))
    head1 = jnp.where(lane < 64, pltpu.roll(trans_a[64:], 64, 1), trans_b[64:])
    return head0, head1


def coded(both):
    i, j = iotas(64, 128)
    on = i == j
    diagonal = jnp.sum(jnp.where(on, both, 0.0), axis=0, keepdims=True)
    high, rest = split2(diagonal)
    low = (diagonal - high.astype(F32) - rest.astype(F32)).astype(BF16)
    row = lax.broadcasted_iota(jnp.int32, (16, 128), 0)
    below = jnp.where(
        row == 0,
        high.astype(F32),
        jnp.where(row == 1, rest.astype(F32), jnp.where(row == 2, low.astype(F32), 0.0)),
    )
    return jnp.concatenate([jnp.where(on, 0.0, both), below], axis=0).astype(BF16)


def decoded(code):
    code = code.astype(F32)
    i, j = iotas(64, 128)
    diagonal = code[64:65] + code[65:66] + code[66:67]
    return jnp.where(i == j, diagonal, code[:64])


def combine(later, total):
    lane = lax.broadcasted_iota(jnp.int32, later.shape, 1)
    return three(later[:, :64], total) + jnp.where(lane < 64, 0.0, later)


FIRST = 256
SECOND = 384


def joined(ref, base, c, first):
    columns = pl.ds(base, first)
    rows = []
    for i in range(N):
        for j in range(N):
            b_ = (1 - c) * i + c * j
            a_ = (1 - c) * j + c * i
            rows.append(ref[b_, a_, :, :, columns].reshape(32, first))
    return jnp.concatenate(rows, axis=0)


def kernel(
    tokens,
    norm_gain,
    w0,
    w1,
    w2,
    w3,
    w4,
    w5,
    w6,
    w7,
    out_scan,
    out_conv,
    key_gain,
    removal_gain,
    removal_bias,
    decay_bias,
    extra,
    scan_norm_gain,
    conv_kernel,
    conv_bias,
    conv_norm_gain,
    out,
    mine1,
    mine2,
    weights,
    later,
    extras,
    norm_gain_v,
    tok,
    normed,
    proj,
    outw0,
    outw1,
    line_y,
    line_z,
    rim,
    conv_in,
    conv_pad,
    stats,
    send_scan,
    send_conv,
    feats_scan,
    feats_conv,
    reads_a,
    reads_b,
    load_sem,
    tok_send,
    tok_recv,
    share_send,
    share_recv,
    wide_sems,
    wide_first,
    wide_plus,
    wide_minus,
    thin_sems,
    thin_first,
    thin_plus,
    thin_minus,
    outw_send,
    outw_recv,
    outw_load,
    outw_cross_send,
    outw_cross_recv,
    y_send,
    y_recv,
    z_send,
    z_recv,
    rim_send,
    rim_recv,
    stats_send,
    stats_recv,
    scan_send,
    scan_recv,
    conv_send,
    conv_recv,
):
    z, y, c, x = (lax.axis_index(n) for n in (*SP, "tp"))
    upper = c == 1

    def at(z_=None, y_=None, c_=None, x_=None):
        pick = lambda a, b: a if b is None else b
        return (pick(z, z_), pick(y, y_), pick(c, c_), pick(x, x_))

    def remote(src, dst, send, recv, where):
        return pltpu.make_async_remote_copy(
            src_ref=src, dst_ref=dst, send_sem=send, recv_sem=recv, device_id=where, device_id_type=MESH
        )

    partner = at(c_=1 - c)
    a = (1 - c) * y + c * z
    b = (1 - c) * z + c * y

    loads = [
        pltpu.make_async_copy(tokens, tok.at[x], load_sem.at[0]),
        pltpu.make_async_copy(extra, extras.at[c], load_sem.at[1]),
        pltpu.make_async_copy(norm_gain, norm_gain_v, load_sem.at[2]),
    ]
    for load in loads:
        load.start()

    barrier = pltpu.get_barrier_semaphore()
    greeted = [partner]
    for k in range(1, N):
        for core in range(2):
            greeted.append(at(y_=lax.rem(y + k, N), c_=core))
            greeted.append(at(z_=lax.rem(z + k, N), c_=core))
    for k in range(1, NX):
        for core in range(2):
            greeted.append(at(x_=lax.rem(x + k, NX), c_=core))
    chip = z * N + y
    before = lax.rem(chip + N * N - 1, N * N)
    after = lax.rem(chip + 1, N * N)
    greeted.append((before // N, lax.rem(before, N), c, x))
    for device in greeted:
        pl.semaphore_signal(barrier, inc=1, device_id=device, device_id_type=MESH)

    lane16 = lax.broadcasted_iota(jnp.int32, (16, 128), 1) < 64

    def halves(left, right):
        left, right = left.astype(F32), right.astype(F32)
        first = jnp.where(lane16, left, pltpu.roll(right, 64, 1))
        return first.astype(BF16), jnp.where(lane16, pltpu.roll(left, 64, 1), right).astype(BF16)

    for k, (left, right) in enumerate(((w1, w2), (w3, w4))):
        for core, part_ in enumerate(halves(left[...], right[...])):
            mine1[core, :, 128 * k : 128 * (k + 1)] = part_
    for k, (left, right) in enumerate(((w0, w5), (w6, w7))):
        for core, part_ in enumerate(halves(left[...], right[...])):
            mine2[core, :, 128 * k : 128 * (k + 1)] = part_
    mine2[0, :, 256:384] = out_scan[...]
    mine2[1, :, 256:384] = out_conv[...]

    pl.semaphore_wait(barrier, len(greeted))

    class Gather:
        def __init__(self, own, ref, sems, first_recv, plus_recv, minus_recv):
            self.own, self.ref, self.first_recv = own, ref, first_recv
            self.first_send, self.second_send, self.keep, self.pair_send = (sems.at[k] for k in range(4))
            self.recvs = {1: plus_recv, -1: minus_recv}

        def start(self):
            for k in (0, 1, 7, 2, 6, 3, 5, 4):
                for core in range(2):
                    a_, b_ = (y, z) if core == 0 else (z, y)
                    target = (z, lax.rem(y + k, N), 0, x) if core == 0 else (lax.rem(z + k, N), y, 1, x)
                    src, dst = self.own.at[core], self.ref.at[b_, a_, c]
                    recv = self.first_recv.at[2 * a_ + c]
                    copy = remote(src, dst, self.first_send if k else self.pair_send, recv, target)
                    if k:
                        copy.start()
                    else:

                        @pl.when(c != core)
                        def _():
                            copy.start()

                        @pl.when(c == core)
                        def _():
                            pltpu.make_async_copy(src, dst, self.keep).start()

        def low(self, h):
            return lax.rem(a // 2 + h, 4) * 2

        def piece(self, h, distance):
            return self.ref.at[lax.rem(b + distance + N, N), pl.ds(self.low(h), 2)]

        def copy(self, h, source, sign, reach):
            piece = self.piece(h, -sign * source)
            recv = self.recvs[sign].at[h * 4 + source + reach - 1]
            k = reach if sign > 0 else N - reach
            target = at(z_=lax.rem(z + (1 - c) * k, N), y_=lax.rem(y + c * k, N))
            return remote(piece, piece, self.second_send, recv, target)

        def collect(self, h):
            for k in range(2):
                a_ = self.low(h) + k
                for core in range(2):
                    piece = self.ref.at[b, a_, core]

                    def wait():
                        recv = self.first_recv.at[2 * a_ + core]
                        remote(piece, piece, self.first_send, recv, partner).wait_recv()

                    if h:
                        wait()
                    else:
                        own = jnp.logical_and(a_ == a, c == core)
                        pl.when(jnp.logical_not(own))(wait)
            if h == 0:
                own = self.ref.at[b, a, c]
                pltpu.make_async_copy(own, own, self.keep).wait()
            for reach in (2, 1):
                for sign in (1, -1):
                    self.copy(h, 0, sign, reach).start()

        def has_far(self, h, sign):
            return (h % 2 == 0) == (sign > 0)

        def arrive(self, h, d, sign):
            self.copy(h, 0, sign, d).wait_recv()

        def relay(self, h):
            for sign in (1, -1):
                self.arrive(h, 2, sign)
                if self.has_far(h, sign):
                    self.copy(h, 2, sign, 2).start()
                self.copy(h, 2, sign, 1).start()

        def near(self, h):
            for sign in (1, -1):
                self.arrive(h, 1, sign)

        def far(self, h):
            for sign in (1, -1):
                if self.has_far(h, sign):
                    self.arrive(h, 4, sign)
                self.arrive(h, 3, sign)

        def drain(self):
            fourteen = self.ref.at[0, pl.ds(0, 7)]
            remote(fourteen, fourteen, self.first_send, self.first_recv.at[0], partner).wait_send()
            single = self.ref.at[0, 7, 0]
            remote(single, single, self.pair_send, self.first_recv.at[0], partner).wait_send()
            most = self.ref.at[pl.ds(0, 7)]
            remote(most, most, self.second_send, self.first_recv.at[0], partner).wait_send()

    wide = Gather(mine1, weights, wide_sems, wide_first, wide_plus, wide_minus)
    thin = Gather(mine2, later, thin_sems, thin_first, thin_plus, thin_minus)
    wide.start()
    for load in loads:
        load.wait()
    tok_copies = [
        remote(tok.at[x], tok.at[x], tok_send.at[k - 1], tok_recv.at[k - 1], at(x_=lax.rem(x + k, NX)))
        for k in (1, 3, 2)
    ]
    for copy in tok_copies:
        copy.start()
    extra_copy = remote(extras.at[c], extras.at[c], share_send.at[0], share_recv.at[0], partner)
    extra_copy.start()
    normed_copy = remote(normed.at[c], normed.at[c], share_send.at[1], share_recv.at[1], partner)

    order = (0, 1, 3, 2)
    for h in order:
        wide.collect(h)
    thin.start()
    for h in order:
        wide.relay(h)
    for copy in tok_copies:
        copy.wait_recv()
    square = jnp.zeros((ROWS, 1), F32)
    for q in range(NX):
        t = tok[q].astype(F32)
        square = square + jnp.sum(t * t, axis=-1, keepdims=True)
    factor = lax.rsqrt(square * (1.0 / MODEL) + 1e-06)
    for q in range(NX):
        t = tok[q].astype(F32)
        columns = slice(q * 512, (q + 1) * 512)
        normed[c, :, columns] = (t * factor * norm_gain_v[:, columns]).astype(BF16)
    normed_copy.start()
    for h in order:
        thin.collect(h)
    for h in order:
        wide.near(h)
    extra_copy.wait_recv()
    normed_copy.wait_recv()
    for h in order:
        wide.far(h)

    lane = lax.broadcasted_iota(jnp.int32, (ROWS, 128), 1) < 64

    def turned(v):
        return pltpu.roll(v, 64, 1)

    def own_head(v):
        low = lax.broadcasted_iota(jnp.int32, v.shape, 1) < 64
        other = turned(v)
        return jnp.where(upper, jnp.where(low, other, v), jnp.where(low, v, other))

    def project(ref, base, width, target):
        w = joined(ref, base, c, width)
        for half in range(2):
            proj[half, :, target : target + width] = jnp.dot(
                normed[half], w, preferred_element_type=F32
            ).astype(BF16)

    def parts(k):
        columns = slice(128 * k, 128 * (k + 1))
        p0, p1 = proj[0, :, columns].astype(F32), proj[1, :, columns].astype(F32)
        return jnp.where(lane, p0, turned(p1)), jnp.where(lane, turned(p0), p1)

    project(weights, 0, FIRST, 0)
    keys, values = parts(0)
    decay_pre, removal_pre = parts(1)
    e0, e1 = extras[0], extras[1]
    own_extra = jnp.where(
        upper, jnp.where(lane, turned(e0), e1), jnp.where(lane, e0, turned(e1))
    )
    blocks = prepared(
        keys,
        values,
        decay_pre,
        removal_pre,
        own_head(key_gain[...]),
        own_head(removal_gain[...]),
        own_head(removal_bias[...]),
        own_head(decay_bias[...]),
        own_extra,
    )
    inverted(blocks)
    half0, half1 = packed_heads(*transition(blocks))
    line_y[y] = coded(combine(half1, half0))
    for k in (4, 3, 5, 2, 6, 1, 7):
        remote(line_y.at[y], line_y.at[y], y_send, y_recv.at[y], at(y_=lax.rem(y + k, N))).start()
    for h in order:
        thin.relay(h)

    lane64 = lax.broadcasted_iota(jnp.int32, (64, 128), 1)
    i, j = iotas(64, 128)
    total = inside = (i == j).astype(F32)
    for k in range(N):

        @pl.when(y != k)
        def _():
            remote(line_y.at[k], line_y.at[k], y_send, y_recv.at[k], partner).wait_recv()

        total = combine(decoded(line_y[k]), total)
        inside = jnp.where(k < y, total, inside)
    line_z[z] = coded(total)
    z_copies = []
    for k in range(N - 1, 0, -1):
        copy = remote(
            line_z.at[z], line_z.at[z], z_send.at[k - 1], z_recv.at[z], at(z_=lax.rem(z + k, N))
        )
        z_copies.append((k, copy))

        @pl.when(z + k < N)
        def _():
            copy.start()

    for h in order:
        thin.near(h)
        thin.far(h)

    def outw_copies(p):
        for k in (1, 3, 2, 0):
            x_ = lax.rem(x + k, NX)
            if p:
                src, dst = later.at[:, pl.ds(2 * x_, 2), :, :, pl.ds(256, 128)], outw1.at[x]
            else:
                src, dst = later.at[pl.ds(2 * x_, 2), :, :, :, pl.ds(256, 128)], outw0.at[x]
            if k:
                yield remote(src, dst, outw_send.at[k - 1], outw_recv.at[k - 1], at(x_=x_))
            else:
                yield pltpu.make_async_copy(src, dst, outw_load)

    for p in range(2):

        @pl.when(c == p)
        def _():
            for copy in outw_copies(p):
                copy.start()

    outw_waits = list(outw_copies(0))

    project(later, 0, 256, 256)
    conv_value, conv_gate = parts(3)
    conv_in[...] = (conv_value * sigmoid(conv_gate)).astype(BF16)
    last = chip == N * N - 1
    start = chip == 0
    rim_copy = remote(
        conv_in.at[pl.ds(ROWS - 32, 32)], rim, rim_send, rim_recv, (after // N, lax.rem(after, N), c, x)
    )

    @pl.when(jnp.logical_not(last))
    def _():
        rim_copy.start()

    recept, gate_pre = parts(2)
    reads_a[...], reads_b[...] = read_parts(blocks, recept)

    @pl.when(start)
    def _():
        rim[...] = jnp.zeros_like(rim)

    @pl.when(jnp.logical_not(start))
    def _():
        rim_copy.wait_recv()

    ending = conv_in[pl.ds(ROWS - 32, 32)].astype(F32)
    conv_pad[pl.ds(0, 32)] = turned(jnp.where(lane[:32], ending, rim[...].astype(F32)))
    conv_pad[pl.ds(32, ROWS)] = conv_in[...].astype(F32)
    taps = own_head(conv_kernel[...])
    filtered = own_head(conv_bias[...]) + taps[0:1] * conv_pad[pl.ds(2, ROWS)]
    for k in range(1, CONV_K):
        filtered = filtered + taps[k : k + 1] * conv_pad[pl.ds(2 + k, ROWS)]
    ones = head_ones()
    near = right_exact(filtered, ones) * (1.0 / 64.0)
    around = right_exact((filtered - near) ** 2, ones)
    spot = lax.broadcasted_iota(jnp.int32, (ROWS, 128), 1) & 63
    table = jnp.where(spot == 0, near, jnp.where(spot == 1, around, 0.0)).T
    stats[x, c, 0:8] = table[0:8]
    stats[x, c, 8:16] = table[64:72]
    conv_pad[pl.ds(0, ROWS)] = filtered

    mates = [(k, core) for k in (1, 3, 2, 0) for core in range(2)]

    def to_mates(copy_of, send, recv):
        copies = []
        for k, core in mates:
            src, dst = copy_of(core)
            copy = remote(src, dst, send.at[2 * k + core], recv.at[2 * k + c], at(x_=lax.rem(x + k, NX), c_=core))
            copies.append((k, core, copy))
        return copies

    def start_all(copies, keep):
        for k, core, copy in copies:
            if k:
                copy.start()
            else:

                @pl.when(c != core)
                def _():
                    copy.start()

                if keep is not None:

                    @pl.when(c == core)
                    def _():
                        keep(core)

    def wait_all(copies, recv):
        for k, core, copy in copies:
            src, dst = copy.src_ref, copy.dst_ref
            arriving = remote(dst, dst, recv.at[2 * k + core], recv.at[2 * k + core], partner)
            if k:
                arriving.wait_recv()
            else:

                @pl.when(c != core)
                def _():
                    arriving.wait_recv()

    def sent_all(copies):
        for k, core, copy in copies:
            if k:
                copy.wait_send()
            else:

                @pl.when(c != core)
                def _():
                    copy.wait_send()

    stats_copies = to_mates(lambda core: (stats.at[x, c], stats.at[x, c]), stats_send, stats_recv)
    start_all(stats_copies, None)

    for copy in outw_waits[:3]:
        copy.wait_recv()
    outw_waits[3].wait()
    for p, ref in enumerate((outw0, outw1)):

        @pl.when(c == p)
        def _():
            remote(ref, ref, outw_cross_send, outw_cross_recv, partner).start()

    wait_all(stats_copies, stats_recv)
    sides = []
    for half in range(2):
        rows = [stats[q, core, 8 * half : 8 * half + 2] for q in range(NX) for core in range(2)]
        center = sum(r[0:1] for r in rows) * (1.0 / 8.0)
        around_row = sum(r[1:2] + 64.0 * (r[0:1] - center) ** 2 for r in rows)
        sides.append((center, lax.rsqrt(around_row * (1.0 / 512.0) + 1e-05)))
    row = lax.broadcasted_iota(jnp.int32, (8, ROWS), 0)
    column = jnp.where(
        row == 0,
        sides[0][0],
        jnp.where(row == 1, sides[0][1], jnp.where(row == 2, sides[1][0], sides[1][1])),
    ).T
    center = jnp.where(lane, column[:, 0:1], column[:, 2:3])
    scale = jnp.where(lane, column[:, 1:2], column[:, 3:4])
    normal = (conv_pad[pl.ds(0, ROWS)] - center) * scale * own_head(conv_norm_gain[...])

    def by_half(v, ref):
        upper_rows, lower_rows = v[:96], v[96:]
        low = lane[:96]
        ref[0] = jnp.where(low, upper_rows, turned(lower_rows)).astype(BF16)
        ref[1] = jnp.where(low, turned(upper_rows), lower_rows).astype(BF16)

    def natural(ref, q):
        f0, f1 = ref[q, 0].astype(F32), ref[q, 1].astype(F32)
        low = lane[:96]
        rows = [jnp.where(low, f0, turned(f1)), jnp.where(low, turned(f0), f1)]
        return jnp.concatenate(rows, axis=0).astype(BF16)

    by_half(normal * sigmoid(normal), send_conv)
    conv_copies = to_mates(lambda core: (send_conv.at[core], feats_conv.at[x, c]), conv_send, conv_recv)

    def keep_conv(core):
        feats_conv[x, c] = send_conv[core]

    start_all(conv_copies, keep_conv)

    def advance(k, state):
        remote(line_z.at[k], line_z.at[k], z_send.at[0], z_recv.at[k], partner).wait_recv()
        return combine(decoded(line_z[k]), state)

    state = lax.fori_loop(0, z, advance, jnp.zeros((64, 128), F32))
    state0 = jnp.where(lane64 < 64, 0.0, combine(inside, state))
    state1 = combine(half0, state0)
    whole = jnp.concatenate(
        [
            jnp.where(lane64 < 64, turned(state0), 0.0),
            jnp.where(lane64 < 64, 0.0, state1),
        ],
        axis=0,
    )
    reads = three(reads_a[...], whole) + reads_b[...]
    reads = reads - right_exact(reads, ones) * (1.0 / 64.0)
    spread_ = right_exact(reads * reads, ones) * (1.0 / 64.0)
    by_half(
        reads * lax.rsqrt(spread_ + 0.00064) * own_head(scan_norm_gain[...]) * sigmoid(gate_pre), send_scan
    )
    scan_copies = to_mates(lambda core: (send_scan.at[core], feats_scan.at[x, c]), scan_send, scan_recv)

    def keep_scan(core):
        feats_scan[x, c] = send_scan[core]

    start_all(scan_copies, keep_scan)

    outw_cross = remote(outw0, outw0, outw_cross_send, outw_cross_recv, partner)
    outw_cross.wait_recv()
    wait_all(conv_copies, conv_recv)

    def w_scan(q):
        return outw0[q].reshape(512, 128)

    def w_conv(q):
        rows = [outw1[q, j, i].reshape(32, 128) for i in range(2) for j in range(N)]
        return jnp.concatenate(rows, axis=0)

    total_out = one_nt(natural(feats_conv, 0), w_conv(0))
    for q in range(1, NX):
        total_out = total_out + one_nt(natural(feats_conv, q), w_conv(q))
    wait_all(scan_copies, scan_recv)
    for q in range(NX):
        total_out = total_out + one_nt(natural(feats_scan, q), w_scan(q))
    out[...] = total_out.astype(BF16)

    for copies in (tok_copies, outw_waits[:3], [extra_copy, normed_copy, outw_cross]):
        for copy in copies:
            copy.wait_send()
    for copies in (stats_copies, conv_copies, scan_copies):
        sent_all(copies)
    wide.drain()
    thin.drain()
    lines = line_y.at[pl.ds(0, 7)]
    remote(lines, lines, y_send, y_recv.at[0], partner).wait_send()

    @pl.when(jnp.logical_not(last))
    def _():
        rim_copy.wait_send()

    for k, copy in z_copies:

        @pl.when(z + k < N)
        def _():
            copy.wait_send()


def shards(
    tokens,
    norm_gain,
    query_weight,
    key_weight,
    value_weight,
    decay_weight,
    removal_weight,
    gate_weight,
    key_gain,
    removal_gain,
    removal_bias,
    decay_bias,
    decay_extra,
    scan_norm_gain,
    conv_value_weight,
    conv_gate_weight,
    conv_kernel,
    conv_bias,
    conv_norm_gain,
    out_scan_weight,
    out_conv_weight,
):
    row = lambda v: v.reshape(1, -1)
    anywhere = pl.BlockSpec(memory_space=pl.ANY)
    inside = pl.BlockSpec(memory_space=pltpu.VMEM)
    dma = pltpu.SemaphoreType.DMA
    vmem = pltpu.VMEM
    return pl.pallas_call(
        kernel,
        out_shape=jax.ShapeDtypeStruct((ROWS, 512), BF16),
        in_specs=[anywhere] * 2 + [inside] * 14 + [anywhere] + [inside] * 4,
        out_specs=inside,
        scratch_shapes=[
            vmem((2, 16, FIRST), BF16),
            vmem((2, 16, SECOND), BF16),
            vmem((N, N, 2, 16, FIRST), BF16),
            vmem((N, N, 2, 16, SECOND), BF16),
            vmem((2, ROWS, 128), F32),
            vmem((1, MODEL), F32),
            vmem((NX, ROWS, 512), BF16),
            vmem((2, ROWS, MODEL), BF16),
            vmem((2, ROWS, 512), BF16),
            vmem((NX, 2, N, 2, 16, 128), BF16),
            vmem((NX, N, 2, 2, 16, 128), BF16),
            vmem((N, 80, 128), BF16),
            vmem((N, 80, 128), BF16),
            vmem((32, 128), BF16),
            vmem((ROWS, 128), BF16),
            vmem((ROWS + 32, 128), F32),
            vmem((NX, 2, 16, ROWS), F32),
            vmem((2, 96, 128), BF16),
            vmem((2, 96, 128), BF16),
            vmem((NX, 2, 96, 128), BF16),
            vmem((NX, 2, 96, 128), BF16),
            vmem((ROWS, 128), F32),
            vmem((ROWS, 128), F32),
            dma((3,)),
            dma((3,)),
            dma((3,)),
            dma((2,)),
            dma((2,)),
            dma((4,)),
            dma((16,)),
            dma((16,)),
            dma((16,)),
            dma((4,)),
            dma((16,)),
            dma((16,)),
            dma((16,)),
            dma((3,)),
            dma((3,)),
            dma(()),
            dma(()),
            dma(()),
            dma(()),
            dma((N,)),
            dma((N - 1,)),
            dma((N,)),
            dma(()),
            dma(()),
            dma((8,)),
            dma((8,)),
            dma((8,)),
            dma((8,)),
            dma((8,)),
            dma((8,)),
        ],
        compiler_params=pltpu.CompilerParams(
            collective_id=0, has_side_effects=True, vmem_limit_bytes=56 * 1024 * 1024
        ),
    )(
        tokens,
        row(norm_gain),
        query_weight,
        key_weight,
        value_weight,
        decay_weight,
        removal_weight,
        gate_weight,
        conv_value_weight,
        conv_gate_weight,
        out_scan_weight.T,
        out_conv_weight.T,
        row(key_gain),
        row(removal_gain),
        row(removal_bias),
        row(decay_bias),
        decay_extra,
        row(scan_norm_gain),
        conv_kernel,
        row(conv_bias),
        row(conv_norm_gain),
    )


def solution(mesh):
    torus = Mesh(mesh.devices.reshape(N, N, 2, mesh.shape["tp"]), (*SP, "tp"))
    in_specs = (
        P(SP, "tp"),
        P(),
        P(SP, "tp"),
        P(SP, "tp"),
        P(SP, "tp"),
        P(SP, "tp"),
        P(SP, "tp"),
        P(SP, "tp"),
        P("tp"),
        P("tp"),
        P("tp"),
        P("tp"),
        P(SP, "tp"),
        P("tp"),
        P(SP, "tp"),
        P(SP, "tp"),
        P(None, "tp"),
        P("tp"),
        P("tp"),
        P("tp", SP),
        P("tp", SP),
    )
    return jax.shard_map(
        shards, mesh=torus, in_specs=in_specs, out_specs=P(SP, "tp"), check_vma=False
    )
```

time: 67.4 us -> 64.6 us (0.958)
  Pallas kernels: 65 us -> 62.8 us
    pallas_call x1, Pallas kernels: 65 us -> 62.8 us  [shards(): pl.pallas_call(kernel, out_shape=jax.ShapeDtypeStruct((ROWS, 512), BF16),...]
where the time goes in v5:
time: 64.6 us; the launch traced here: 64.4 us
  Pallas kernels  62.8 us (97%)
  local copies, waits for them, and re-layouts  1.62 us (3%)
    pallas_call x1, Pallas kernels, shards(): pl.pallas_call(kernel, out_shape=jax.ShapeDtypeStruct((ROWS, 512), BF16),...  62.8 us
    unnamed x1, local copies, waits for them, and re-layouts  1.62 us

profile of v5, /device:TPU:1, one launch (start us, length us, event | category | flops | bytes accessed | tf_op | source)
XLA Modules:
  0.0 64.4 jit_solution(4774435605137611812)
XLA Ops:
  0.0 62.8 %shard_map.199 = bf16[192,512]{1,0:T(8,128)(2,1)} custom-call(bf16[192,512]{1,0:T(8,128)(2,1)} %tokens.1, f32[1,2048]{1,0:T(1,128)} %bitcast.10, bf16[16,128]{1,0:T(8,128)(2,1)} %w0.1, bf16[16,128]{1,0:T(8,128)(2,1)} %w1.1, bf16[16,128]{1,0:T(8,128)(2,1)} %w2.1, bf16[16,128]{1,0:T(8,128)(2,1)} %w3.1, bf16[16,128]{1,0:T(8,128)(2,1)} %w4.1, ...), custom_call_target="tpu_custom_call" | custom-call | tf_op jit(solution)/shard_map/pallas_call | solution.py:851
  62.8 1.6 %copy.23 = bf16[192,512]{1,0:T(8,128)(2,1)} copy(bf16[192,512]{1,0:T(8,128)(2,1)} %shard_map.199) | data formatting | bytes 393216

commit v6 on v5

--- a/solution.py
+++ b/solution.py
@@ -237,7 +237,8 @@
 
 
 FIRST = 256
-SECOND = 384
+SECOND = 256
+THIRD = 128
 
 
 def joined(ref, base, c, first):
@@ -276,8 +277,10 @@
     out,
     mine1,
     mine2,
+    mine3,
     weights,
     later,
+    last_w,
     extras,
     norm_gain_v,
     tok,
@@ -310,6 +313,10 @@
     thin_first,
     thin_plus,
     thin_minus,
+    third_sems,
+    third_first,
+    third_plus,
+    third_minus,
     outw_send,
     outw_recv,
     outw_load,
@@ -378,11 +385,12 @@
     for k, (left, right) in enumerate(((w1, w2), (w3, w4))):
         for core, part_ in enumerate(halves(left[...], right[...])):
             mine1[core, :, 128 * k : 128 * (k + 1)] = part_
-    for k, (left, right) in enumerate(((w0, w5), (w6, w7))):
-        for core, part_ in enumerate(halves(left[...], right[...])):
-            mine2[core, :, 128 * k : 128 * (k + 1)] = part_
-    mine2[0, :, 256:384] = out_scan[...]
-    mine2[1, :, 256:384] = out_conv[...]
+    for core, part_ in enumerate(halves(w6[...], w7[...])):
+        mine2[core, :, 0:128] = part_
+    for core, part_ in enumerate(halves(w0[...], w5[...])):
+        mine3[core] = part_
+    mine2[0, :, 128:256] = out_scan[...]
+    mine2[1, :, 128:256] = out_conv[...]
 
     pl.semaphore_wait(barrier, len(greeted))
 
@@ -480,6 +488,7 @@
 
     wide = Gather(mine1, weights, wide_sems, wide_first, wide_plus, wide_minus)
     thin = Gather(mine2, later, thin_sems, thin_first, thin_plus, thin_minus)
+    third = Gather(mine3, last_w, third_sems, third_first, third_plus, third_minus)
     wide.start()
     for load in loads:
         load.wait()
@@ -499,6 +508,7 @@
     thin.start()
     for h in order:
         wide.relay(h)
+    third.start()
     for copy in tok_copies:
         copy.wait_recv()
     square = jnp.zeros((ROWS, 1), F32)
@@ -567,30 +577,8 @@
         remote(line_y.at[y], line_y.at[y], y_send, y_recv.at[y], at(y_=lax.rem(y + k, N))).start()
     for h in order:
         thin.relay(h)
-
-    lane64 = lax.broadcasted_iota(jnp.int32, (64, 128), 1)
-    i, j = iotas(64, 128)
-    total = inside = (i == j).astype(F32)
-    for k in range(N):
-
-        @pl.when(y != k)
-        def _():
-            remote(line_y.at[k], line_y.at[k], y_send, y_recv.at[k], partner).wait_recv()
-
-        total = combine(decoded(line_y[k]), total)
-        inside = jnp.where(k < y, total, inside)
-    line_z[z] = coded(total)
-    z_copies = []
-    for k in range(N - 1, 0, -1):
-        copy = remote(
-            line_z.at[z], line_z.at[z], z_send.at[k - 1], z_recv.at[z], at(z_=lax.rem(z + k, N))
-        )
-        z_copies.append((k, copy))
-
-        @pl.when(z + k < N)
-        def _():
-            copy.start()
-
+    for h in order:
+        third.collect(h)
     for h in order:
         thin.near(h)
         thin.far(h)
@@ -599,9 +587,9 @@
         for k in (1, 3, 2, 0):
             x_ = lax.rem(x + k, NX)
             if p:
-                src, dst = later.at[:, pl.ds(2 * x_, 2), :, :, pl.ds(256, 128)], outw1.at[x]
+                src, dst = later.at[:, pl.ds(2 * x_, 2), :, :, pl.ds(128, 128)], outw1.at[x]
             else:
-                src, dst = later.at[pl.ds(2 * x_, 2), :, :, :, pl.ds(256, 128)], outw0.at[x]
+                src, dst = later.at[pl.ds(2 * x_, 2), :, :, :, pl.ds(128, 128)], outw0.at[x]
             if k:
                 yield remote(src, dst, outw_send.at[k - 1], outw_recv.at[k - 1], at(x_=x_))
             else:
@@ -616,7 +604,7 @@
 
     outw_waits = list(outw_copies(0))
 
-    project(later, 0, 256, 256)
+    project(later, 0, 128, 384)
     conv_value, conv_gate = parts(3)
     conv_in[...] = (conv_value * sigmoid(conv_gate)).astype(BF16)
     last = chip == N * N - 1
@@ -629,8 +617,36 @@
     def _():
         rim_copy.start()
 
-    recept, gate_pre = parts(2)
-    reads_a[...], reads_b[...] = read_parts(blocks, recept)
+    lane64 = lax.broadcasted_iota(jnp.int32, (64, 128), 1)
+    i, j = iotas(64, 128)
+    nothing = (i == j).astype(F32)
+    for k in range(N):
+
+        @pl.when(y != k)
+        def _():
+            remote(line_y.at[k], line_y.at[k], y_send, y_recv.at[k], partner).wait_recv()
+
+    each = [decoded(line_y[k]) for k in range(N)]
+    pairs = [combine(each[2 * k + 1], each[2 * k]) for k in range(4)]
+    quads = [combine(pairs[1], pairs[0]), combine(pairs[3], pairs[2])]
+    line_z[z] = coded(combine(quads[1], quads[0]))
+    z_copies = []
+    for k in range(N - 1, 0, -1):
+        copy = remote(
+            line_z.at[z], line_z.at[z], z_send.at[k - 1], z_recv.at[z], at(z_=lax.rem(z + k, N))
+        )
+        z_copies.append((k, copy))
+
+        @pl.when(z + k < N)
+        def _():
+            copy.start()
+
+    for h in order:
+        third.relay(h)
+    inside = jnp.where(y >= 4, quads[0], nothing)
+    inside = jnp.where(lax.rem(y, 4) >= 2, combine(jnp.where(y >= 4, pairs[2], pairs[0]), inside), inside)
+    previous = decoded(line_y[jnp.maximum(y - 1, 0)])
+    inside = jnp.where(lax.rem(y, 2) == 1, combine(previous, inside), inside)
 
     @pl.when(start)
     def _():
@@ -706,6 +722,13 @@
 
     stats_copies = to_mates(lambda core: (stats.at[x, c], stats.at[x, c]), stats_send, stats_recv)
     start_all(stats_copies, None)
+
+    for h in order:
+        third.near(h)
+        third.far(h)
+    project(last_w, 0, 128, 256)
+    recept, gate_pre = parts(2)
+    reads_a[...], reads_b[...] = read_parts(blocks, recept)
 
     for copy in outw_waits[:3]:
         copy.wait_recv()
@@ -753,11 +776,16 @@
 
     start_all(conv_copies, keep_conv)
 
-    def advance(k, state):
-        remote(line_z.at[k], line_z.at[k], z_send.at[0], z_recv.at[k], partner).wait_recv()
-        return combine(decoded(line_z[k]), state)
-
-    state = lax.fori_loop(0, z, advance, jnp.zeros((64, 128), F32))
+    for k in range(N - 1):
+
+        @pl.when(k < z)
+        def _():
+            remote(line_z.at[k], line_z.at[k], z_send.at[0], z_recv.at[k], partner).wait_recv()
+
+    each = [jnp.where(k < z, decoded(line_z[k]), nothing) for k in range(N - 1)]
+    pairs = [combine(each[2 * k + 1], each[2 * k]) for k in range(3)]
+    state = combine(combine(each[6], pairs[2]), combine(pairs[1], pairs[0]))
+    state = jnp.where(lane64 < 64, 0.0, state)
     state0 = jnp.where(lane64 < 64, 0.0, combine(inside, state))
     state1 = combine(half0, state0)
     whole = jnp.concatenate(
@@ -806,6 +834,7 @@
         sent_all(copies)
     wide.drain()
     thin.drain()
+    third.drain()
     lines = line_y.at[pl.ds(0, 7)]
     remote(lines, lines, y_send, y_recv.at[0], partner).wait_send()
 
@@ -856,8 +885,10 @@
         scratch_shapes=[
             vmem((2, 16, FIRST), BF16),
             vmem((2, 16, SECOND), BF16),
+            vmem((2, 16, THIRD), BF16),
             vmem((N, N, 2, 16, FIRST), BF16),
             vmem((N, N, 2, 16, SECOND), BF16),
+            vmem((N, N, 2, 16, THIRD), BF16),
             vmem((2, ROWS, 128), F32),
             vmem((1, MODEL), F32),
             vmem((NX, ROWS, 512), BF16),
@@ -882,6 +913,10 @@
             dma((3,)),
             dma((2,)),
             dma((2,)),
+            dma((4,)),
+            dma((16,)),
+            dma((16,)),
+            dma((16,)),
             dma((4,)),
             dma((16,)),
             dma((16,)),

time: 64.6 us -> 62.5 us (0.967)
  Pallas kernels: 62.8 us -> 60.7 us
    pallas_call x1, Pallas kernels: 62.8 us -> 60.7 us  [shards(): pl.pallas_call(kernel, out_shape=jax.ShapeDtypeStruct((ROWS, 512), BF16),...]
where the time goes in v6:
time: 62.5 us; the launch traced here: 62.3 us
  Pallas kernels  60.7 us (97%)
  local copies, waits for them, and re-layouts  1.62 us (3%)
    pallas_call x1, Pallas kernels, shards(): pl.pallas_call(kernel, out_shape=jax.ShapeDtypeStruct((ROWS, 512), BF16),...  60.7 us
    unnamed x1, local copies, waits for them, and re-layouts  1.62 us

profile of v6, /device:TPU:1, one launch (start us, length us, event | category | flops | bytes accessed | tf_op | source)
XLA Modules:
  0.0 62.3 jit_solution(8425846905415944256)
XLA Ops:
  0.0 60.7 %shard_map.199 = bf16[192,512]{1,0:T(8,128)(2,1)} custom-call(bf16[192,512]{1,0:T(8,128)(2,1)} %tokens.1, f32[1,2048]{1,0:T(1,128)} %bitcast.10, bf16[16,128]{1,0:T(8,128)(2,1)} %w0.1, bf16[16,128]{1,0:T(8,128)(2,1)} %w1.1, bf16[16,128]{1,0:T(8,128)(2,1)} %w2.1, bf16[16,128]{1,0:T(8,128)(2,1)} %w3.1, bf16[16,128]{1,0:T(8,128)(2,1)} %w4.1, ...), custom_call_target="tpu_custom_call" | custom-call | tf_op jit(solution)/shard_map/pallas_call | solution.py:880
  60.7 1.6 %copy.23 = bf16[192,512]{1,0:T(8,128)(2,1)} copy(bf16[192,512]{1,0:T(8,128)(2,1)} %shard_map.199) | data formatting | bytes 393216

commit v7 on v6

--- a/solution.py
+++ b/solution.py
@@ -334,6 +334,10 @@
     scan_recv,
     conv_send,
     conv_recv,
+    small_w,
+    small_v,
+    small_k,
+    small_sem,
 ):
     z, y, c, x = (lax.axis_index(n) for n in (*SP, "tp"))
     upper = c == 1
@@ -356,8 +360,22 @@
         pltpu.make_async_copy(extra, extras.at[c], load_sem.at[1]),
         pltpu.make_async_copy(norm_gain, norm_gain_v, load_sem.at[2]),
     ]
-    for load in loads:
+    sources = [w0, w1, w2, w3, w4, w5, w6, w7, out_scan, out_conv]
+    vectors = [key_gain, removal_gain, removal_bias, decay_bias, scan_norm_gain, conv_bias, conv_norm_gain]
+    weight_loads = [
+        pltpu.make_async_copy(ref, small_w.at[k], small_sem.at[k]) for k, ref in enumerate(sources)
+    ]
+    loads += [
+        pltpu.make_async_copy(ref, small_v.at[k], small_sem.at[10 + k]) for k, ref in enumerate(vectors)
+    ]
+    loads.append(pltpu.make_async_copy(conv_kernel, small_k, small_sem.at[17]))
+    for load in weight_loads + loads:
         load.start()
+    w0, w1, w2, w3, w4, w5, w6, w7, out_scan, out_conv = (small_w.at[k] for k in range(10))
+    key_gain, removal_gain, removal_bias, decay_bias, scan_norm_gain, conv_bias, conv_norm_gain = (
+        small_v.at[k] for k in range(7)
+    )
+    conv_kernel = small_k
 
     barrier = pltpu.get_barrier_semaphore()
     greeted = [partner]
@@ -375,6 +393,8 @@
     for device in greeted:
         pl.semaphore_signal(barrier, inc=1, device_id=device, device_id_type=MESH)
 
+    for load in weight_loads:
+        load.wait()
     lane16 = lax.broadcasted_iota(jnp.int32, (16, 128), 1) < 64
 
     def halves(left, right):
@@ -880,7 +900,7 @@
     return pl.pallas_call(
         kernel,
         out_shape=jax.ShapeDtypeStruct((ROWS, 512), BF16),
-        in_specs=[anywhere] * 2 + [inside] * 14 + [anywhere] + [inside] * 4,
+        in_specs=[anywhere] * 21,
         out_specs=inside,
         scratch_shapes=[
             vmem((2, 16, FIRST), BF16),
@@ -942,6 +962,10 @@
             dma((8,)),
             dma((8,)),
             dma((8,)),
+            vmem((10, 16, 128), BF16),
+            vmem((7, 1, 128), F32),
+            vmem((CONV_K, 128), F32),
+            dma((18,)),
         ],
         compiler_params=pltpu.CompilerParams(
             collective_id=0, has_side_effects=True, vmem_limit_bytes=56 * 1024 * 1024

time: 62.5 us -> 61.8 us (0.989)
    pallas_call x1, Pallas kernels: 60.7 us -> 60.1 us  [shards(): pl.pallas_call(kernel, out_shape=jax.ShapeDtypeStruct((ROWS, 512), BF16),...]
where the time goes in v7:
time: 61.8 us; the launch traced here: 61.7 us
  Pallas kernels  60.1 us (97%)
  local copies, waits for them, and re-layouts  1.62 us (3%)
    pallas_call x1, Pallas kernels, shards(): pl.pallas_call(kernel, out_shape=jax.ShapeDtypeStruct((ROWS, 512), BF16),...  60.1 us
    unnamed x1, local copies, waits for them, and re-layouts  1.62 us

profile of v7, /device:TPU:1, one launch (start us, length us, event | category | flops | bytes accessed | tf_op | source)
XLA Modules:
  0.0 61.7 jit_solution(9183034464411791296)
XLA Ops:
  0.0 60.1 %shard_map.199 = bf16[192,512]{1,0:T(8,128)(2,1)} custom-call(bf16[192,512]{1,0:T(8,128)(2,1)} %tokens.1, f32[1,2048]{1,0:T(1,128)} %bitcast.10, bf16[16,128]{1,0:T(8,128)(2,1)} %w0.1, bf16[16,128]{1,0:T(8,128)(2,1)} %w1.1, bf16[16,128]{1,0:T(8,128)(2,1)} %w2.1, bf16[16,128]{1,0:T(8,128)(2,1)} %w3.1, bf16[16,128]{1,0:T(8,128)(2,1)} %w4.1, ...), custom_call_target="tpu_custom_call" | custom-call | tf_op jit(solution)/shard_map/pallas_call | solution.py:900
  60.1 1.6 %copy.23 = bf16[192,512]{1,0:T(8,128)(2,1)} copy(bf16[192,512]{1,0:T(8,128)(2,1)} %shard_map.199) | data formatting | bytes 393216
